TPU v7x, 256 devices: a whole 4x4x8 slice. The times are simulated.
256 devices in a mesh: sp: 16 (over y, x), tp: 16 (over z, core).
Axes of the slice: x: 4, y: 4, z: 8, core: 2. Of those that a mesh axis runs over, the one named last changes fastest.
Arguments:
- upstream: bfloat16 [4096, 4096], P('sp', 'tp'), may hold values from -6 to 6
- stream: bfloat16 [4096, 4096], P('sp', 'tp'), may hold values from -400 to 400
- norm_gain: float32 [4096], P('tp'), may hold values from 0.1 to 1.9
- routes: int32 [4096, 2], P('sp'), may hold values from 0 to 15, all different within a row; in each aligned block of 256 rows (0 to 255, 256 to 511, ...) at most 48 rows name the same one
- route_weights: float32 [4096, 2], P('sp'), may hold values from 0.1 to 1
- w_gate: bfloat16 [16, 4096, 2048], P('sp', None, 'tp'), may hold values from -0.09375 to 0.09375
- w_up: bfloat16 [16, 4096, 2048], P('sp', None, 'tp'), may hold values from -0.09375 to 0.09375
- w_down: bfloat16 [16, 2048, 4096], P('sp', 'tp'), may hold values from -0.125 to 0.125
- value_in: bfloat16 [4096, 2048], P('sp', 'tp'), may hold values from -6 to 6
- gate_in: bfloat16 [4096, 2048], P('sp', 'tp'), may hold values from -6 to 6
- conv_pre: bfloat16 [4096, 2048], P('sp', 'tp'), may hold values from -200 to 200
- ln_gain: float32 [2048], P('tp'), may hold values from 0.1 to 1.9
- conv_taps: float32 [31, 2048], P(None, 'tp'), may hold values from -1 to 1
- w_out: bfloat16 [2048, 4096], P('tp'), may hold values from -0.125 to 0.125
Outputs:
- grad_gate: float32 [16, 4096, 2048], P('sp', None, 'tp')
- grad_up: float32 [16, 4096, 2048], P('sp', None, 'tp')
- grad_down: float32 [16, 2048, 4096], P('sp', 'tp')
- grad_out: float32 [2048, 4096], P('tp', 'sp')
- value_grad: bfloat16 [4096, 2048], P('sp', 'tp')
- gate_grad: bfloat16 [4096, 2048], P('sp', 'tp')
Inputs may be any that keep to these rules, and one draw needn't show every extreme that they name: `routes`: each token names two different experts. Among the tokens of one index of sp no expert is named more than 48 times, and in every draw some expert exactly 48 times.
All inputs are finite; a program needn't handle non-finite values.
Results may differ from a plain program's by a relative error of at most 0.0071.
Values may be sent and summed in bfloat16 or wider, within the bound.
No kernel may reach another device: no remote copies, remote signals or barrier semaphores. Data moves between devices by JAX's collectives and lax.ppermute only.
A program may use at most 128 MiB of HBM per device.

v0:
```python
import jax
import jax.numpy as jnp
from jax import lax
from jax.experimental import pallas as pl
from jax.experimental.pallas import tpu as pltpu
from jax.sharding import Mesh, PartitionSpec as P

EPSILON = 1e-06
TP = ("z", "c")
BF = jnp.bfloat16
F4 = jnp.float32


def of_everyone(value):
    count = 16
    everything = lax.all_to_all(
        jnp.broadcast_to(value[None], (count, *value.shape)), TP, 0, 0, tiled=True
    )
    return jnp.sum(everything, axis=0)


def in_one(arrays):
    total = of_everyone(jnp.concatenate([a.reshape(-1) for a in arrays]))
    out, at = [], 0
    for a in arrays:
        out.append(total[at : at + a.size].reshape(a.shape))
        at += a.size
    return out


def right(x):
    n = lax.axis_size("z")
    return lax.ppermute(x, "z", [(i, (i + 1) % n) for i in range(n)])


def left(x):
    n = lax.axis_size("z")
    return lax.ppermute(x, "z", [(i, (i - 1) % n) for i in range(n)])


def hops(x, n_hops):
    n = lax.axis_size("z")
    return lax.ppermute(x, "z", [(i, (i + n_hops) % n) for i in range(n)])


def swap(x):
    return lax.ppermute(x, "c", [(0, 1), (1, 0)])


def silu_slope(values):
    logistic = jax.nn.sigmoid(values)
    return logistic * (1.0 + values * (1.0 - logistic))


def dot(a, b, ca, cb):
    return lax.dot_general(a, b, (((ca,), (cb,)), ((), ())), preferred_element_type=F4)


VMEM = pl.BlockSpec(memory_space=pltpu.VMEM)
ANY = pl.BlockSpec(memory_space=pl.ANY)
HBM = pl.BlockSpec(memory_space=pltpu.HBM)
SMEM = pl.BlockSpec(memory_space=pltpu.SMEM)
BIG = pltpu.CompilerParams(vmem_limit_bytes=40 * 2**20)


def scatter_body(
    routes_h, weights_h, upstream_h, stream_h, picker, sent, *scratch, experts, capacity
):
    routes, weights, upstream, stream, sems = scratch
    load_all(
        [(routes_h, routes), (weights_h, weights), (upstream_h, upstream), (stream_h, stream)],
        sems,
    )
    toks = upstream.shape[0]
    slots = experts * capacity
    half = capacity // 2
    r0, r1 = routes[0:1, :], routes[1:2, :]
    names = lax.broadcasted_iota(jnp.int32, (experts, toks), 0)
    hot0 = jnp.where(names == r0, 1.0, 0.0)
    hot1 = jnp.where(names == r1, 1.0, 0.0)
    earlier = jnp.where(
        lax.broadcasted_iota(jnp.int32, (toks, toks), 0)
        < lax.broadcasted_iota(jnp.int32, (toks, toks), 1),
        1.0,
        0.0,
    ).astype(BF)
    before = dot((hot0 + hot1).astype(BF), earlier, 1, 0)
    slot0 = r0 * capacity + jnp.sum(before * hot0, axis=0, keepdims=True).astype(jnp.int32)
    slot1 = r1 * capacity + jnp.sum(before * hot1, axis=0, keepdims=True).astype(jnp.int32)
    blocks = 4
    step = blocks * capacity

    def rows_at(j, carry):
        at = j * (step // 2)
        ids = lax.broadcasted_iota(jnp.int32, (step // 2, toks), 0) + at
        one = jnp.where(ids == slot0, 1.0, 0.0) + jnp.where(ids == slot1, 1.0, 0.0)
        picker[pl.ds(pl.multiple_of(at, step // 2), step // 2), :] = one.astype(BF)
        wide = lax.broadcasted_iota(jnp.int32, (step, toks), 0)
        block = lax.shift_right_logical(wide * (65536 // capacity + 1), 16)
        place = wide - block * capacity
        ids = jnp.where(place >= half, place - half, place) + (block + j * blocks) * half
        hit0, hit1 = ids == slot0, ids == slot1
        pick = (jnp.where(hit0, 1.0, 0.0) + jnp.where(hit1, 1.0, 0.0)).astype(BF)
        weight = jnp.sum(
            jnp.where(hit0, weights[0:1, :], 0.0) + jnp.where(hit1, weights[1:2, :], 0.0),
            axis=1,
            keepdims=True,
        )
        is_cot = place[:, 0:1] >= half
        value = jnp.where(
            is_cot, dot(pick, upstream[...], 1, 0) * weight, dot(pick, stream[...], 1, 0)
        )
        sent[pl.ds(pl.multiple_of(j * step, step), step), :] = value.astype(BF)
        return carry

    lax.fori_loop(0, 2 * slots // step, rows_at, 0)


def offset_of(k, offsets, n):
    off = jnp.int32(0)
    for i, value in enumerate(offsets):
        off = jnp.where(k == i, value % n, off)
    return off


def load_all(pairs, sems):
    copies = [pltpu.make_async_copy(a, b, sems.at[i]) for i, (a, b) in enumerate(pairs)]
    for copy in copies:
        copy.start()
    for copy in copies:
        copy.wait()


def loaded(groups, sems, step):
    copies, at = [], 0
    for group in groups:
        copies.append([])
        for a, b in group:
            copies[-1].append(pltpu.make_async_copy(a, b, sems.at[at]))
            at += 1
    for group in copies:
        for copy in group:
            copy.start()
    for group in copies:
        for copy in group:
            copy.wait()
    lax.fori_loop(0, len(groups), step, 0)


def unpack_body(arrived, x, c, *, n_sp):
    half = x.shape[0] // n_sp
    width = arrived.shape[1]
    for s in range(0, n_sp, 2):
        for core in range(2):
            pair = []
            for src in (s, s + 1):
                at = (2 * src + core) * 2 * half
                pair.append(arrived[at : at + 2 * half, :].astype(F4))
            lanes = pl.ds(core * width, width)
            to = pl.ds(s * half, 2 * half)
            x[to, lanes] = jnp.concatenate([p[:half] for p in pair], axis=0).astype(BF)
            c[to, lanes] = jnp.concatenate([p[half:] for p in pair], axis=0).astype(BF)


def project_body(z, *refs, offsets, n, more):
    m = len(offsets)
    xb, cb, refs = refs[:m], refs[m : 2 * m], refs[2 * m :]
    guo, gux, dno, dnx, gains, inv = refs[:6]
    starts, refs = (refs[6:9], refs[9:]) if more else (None, refs[6:])
    own, oth, back, xs = refs[:4]
    xbuf, cbuf, xs_v, own_v, oth_v, dno_v, dnx_v, sems = refs[4:]
    rows, width = own.shape[0], xbuf.shape[2]
    hid = back.shape[1] // 2
    groups = []
    for i, off in enumerate(offsets):
        at = pl.multiple_of(lax.rem(z[0] + off % n, n) * width, width)
        groups.append(
            [
                (xb[i], xbuf.at[i]),
                (cb[i], cbuf.at[i]),
                (guo.at[pl.ds(at, width), :], own_v.at[i]),
                (gux.at[pl.ds(at, width), :], oth_v.at[i]),
                (dno.at[:, pl.ds(at, width)], dno_v.at[i]),
                (dnx.at[:, pl.ds(at, width)], dnx_v.at[i]),
            ]
        )
    for i, total in enumerate((own, oth, back)):
        total[...] = starts[i][...] if more else jnp.zeros(total.shape, F4)

    def step(k, carry):
        chip = lax.rem(z[0] + offset_of(k, offsets, n), n)
        x = xbuf[k].astype(F4)
        x = (gains[pl.ds(chip, 1), :] * x * inv[...]).astype(BF)
        xs_v[pl.ds(pl.multiple_of(k * rows, rows), rows), :] = x
        own[...] += dot(x, own_v[k], 1, 0)
        oth[...] += dot(x, oth_v[k], 1, 0)
        c = cbuf[k]
        back[:, :hid] += dot(c, dno_v[k], 1, 1)
        back[:, hid:] += dot(c, dnx_v[k], 1, 1)
        return carry

    loaded(groups, sems, step)
    load_all([(xs_v, xs)], sems)


def project(z, xb, cb, weights, gains, inv, offsets, n, starts):
    rows, wide = xb[0].shape
    m, hid = len(xb), weights[2].shape[0]
    total = jax.ShapeDtypeStruct((rows, 2 * hid), F4)
    return pl.pallas_call(
        lambda *r: project_body(*r, offsets=offsets, n=n, more=starts is not None),
        out_shape=(total, total, total, jax.ShapeDtypeStruct((m * rows, wide), BF)),
        in_specs=[SMEM] + [ANY] * (2 * m + 4) + [VMEM] * (2 + len(starts or ())),
        out_specs=(VMEM, VMEM, VMEM, ANY),
        scratch_shapes=[
            pltpu.VMEM((m, rows, wide), BF),
            pltpu.VMEM((m, rows, wide), BF),
            pltpu.VMEM((m * rows, wide), BF),
            pltpu.VMEM((m, wide, 2 * hid), BF),
            pltpu.VMEM((m, wide, 2 * hid), BF),
            pltpu.VMEM((m, hid, wide), BF),
            pltpu.VMEM((m, hid, wide), BF),
            pltpu.SemaphoreType.DMA((6 * m,)),
        ],
        compiler_params=BIG,
        name="project",
    )(z, *xb, *cb, *weights, gains, inv, *(starts or ()))


def in_parts(row):
    hi = row.astype(BF).astype(F4)
    mid = (row - hi).astype(BF).astype(F4)
    low = (row - hi - mid).astype(BF).astype(F4)
    return hi, mid, low


def part_rows(row):
    hi, mid, low = in_parts(row)
    shape = (16, row.shape[1])
    at = lax.broadcasted_iota(jnp.int32, shape, 0)
    rows = jnp.where(at == 0, hi, jnp.where(at == 1, mid, jnp.where(at == 2, low, 0.0)))
    return rows.astype(BF)


def whole_row(rows):
    rows = rows.astype(F4)
    return rows[0:1] + rows[1:2] + rows[2:3]


def finish_body(z, xf, cf, guo, gux, dno, dnx, gains, inv, own, oth, back, *refs, n):
    hbm, refs = refs[:5], refs[5:]
    along, send_r, send_l = refs[:3]
    held = refs[3:8]
    x4, b_own, b_oth, a_own, a_oth = held
    own_v, oth_v, dno_v, dnx_v, sems = refs[8:]
    rows, width = xf.shape
    hid = dno.shape[0]
    chip = lax.rem(z[0] + n // 2, n)
    at = pl.multiple_of(chip * width, width)
    load_all(
        [
            (guo.at[pl.ds(at, width), :], own_v),
            (gux.at[pl.ds(at, width), :], oth_v),
            (dno.at[:, pl.ds(at, width)], dno_v),
            (dnx.at[:, pl.ds(at, width)], dnx_v),
        ],
        sems,
    )
    x = (gains[pl.ds(chip, 1), :] * xf[...].astype(F4) * inv[...]).astype(BF)
    x4[...] = x
    total = jnp.zeros((rows, 1), F4)
    for pre, w_v, d_v, lo, backs, act in (
        (own, own_v, dno_v, 0, b_own, a_own),
        (oth, oth_v, dnx_v, hid, b_oth, a_oth),
    ):
        both = pre[...] + dot(x, w_v[...], 1, 0)
        gate, upper = both[:, :hid], both[:, hid:]
        ab = back[:, lo : lo + hid] + dot(cf[...], d_v[...], 1, 1)
        sig = jax.nn.sigmoid(gate)
        silu = gate * sig
        act[...] = (silu * upper).astype(BF)
        gb = (ab * upper * (sig * (1.0 + gate * (1.0 - sig)))).astype(BF)
        ub = (ab * silu).astype(BF)
        backs[:, :hid] = gb
        backs[:, hid:] = ub
        total = total + jnp.sum(
            gb.astype(F4) * gate + ub.astype(F4) * upper, axis=1, keepdims=True
        )
    copies = [
        pltpu.make_async_copy(a, b, sems.at[i]) for i, (a, b) in enumerate(zip(held, hbm))
    ]
    for copy in copies:
        copy.start()
    row = jnp.broadcast_to(total, (rows, 128)).T[0:8, :]
    along[:, :rows] = row
    along[:, rows:] = jnp.zeros((8, width - rows), F4)
    part = dot(b_own[...], own_v[...], 1, 1) + dot(b_oth[...], oth_v[...], 1, 1)
    hr = rows // 2
    send_r[:hr, :] = part[:hr].astype(BF)
    send_r[hr:, :] = part_rows(along[0:1, :])
    send_l[...] = part[hr:].astype(BF)
    for copy in copies:
        copy.wait()


def parts_body(b_own, b_oth, guo, gux, out, guo_v, gux_v, sems, *, n):
    width = guo.shape[0] // n

    def copies(k):
        at = pl.ds(pl.multiple_of(k * width, width), width)
        return (
            pltpu.make_async_copy(guo.at[at, :], guo_v.at[at, :], sems.at[2 * k]),
            pltpu.make_async_copy(gux.at[at, :], gux_v.at[at, :], sems.at[2 * k + 1]),
        )

    def begin(k, carry):
        for copy in copies(k):
            copy.start()
        return carry

    def step(k, carry):
        for copy in copies(k):
            copy.wait()
        at = pl.ds(pl.multiple_of(k * width, width), width)
        out[:, at] = (
            dot(b_own[...], guo_v[at, :], 1, 1) + dot(b_oth[...], gux_v[at, :], 1, 1)
        ).astype(BF)
        return carry

    lax.fori_loop(0, n, begin, 0)
    lax.fori_loop(0, n, step, 0)


def hop_body(z, parts, along, ra, la, out_r, out_l, *, k, n, first):
    rows = parts.shape[0]
    width = out_r.shape[1]
    hr = rows // 2

    def block(j):
        at = pl.multiple_of(lax.rem(z[0] + (j + n), n) * width, width)
        return parts[:, pl.ds(at, width)].astype(F4)

    own = along[0:1, :]
    pr, pl_ = block(k), block(-k)
    if first:
        out_r[:hr, :] = (pr[:hr] + ra[:hr, :].astype(F4)).astype(BF)
        out_r[hr:rows, :] = pr[hr:].astype(BF)
        out_r[rows:, :] = part_rows(own + whole_row(ra[hr:, :]))
        out_l[:hr, :] = pl_[:hr].astype(BF)
        out_l[hr:rows, :] = (pl_[hr:] + la[...].astype(F4)).astype(BF)
        out_l[rows:, :] = part_rows(own)
    else:
        out_r[:rows, :] = (pr + ra[:rows, :].astype(F4)).astype(BF)
        out_r[rows:, :] = part_rows(own + whole_row(ra[rows:, :]))
        out_l[:rows, :] = (pl_ + la[:rows, :].astype(F4)).astype(BF)
        out_l[rows:, :] = part_rows(own + whole_row(la[rows:, :]))


def pack_body(z, parts, along, ra, la, out, value, extra, *, n_sp):
    rows = parts.shape[0]
    width = ra.shape[1]
    half = width // 2
    step = rows // n_sp
    at = pl.multiple_of(z[0] * width, width)
    row = along[0:1, :] + whole_row(ra[rows:, :]) + whole_row(la[rows:, :])
    col = jnp.broadcast_to(row[:, :rows], (128, rows)).T
    hi, mid, low = in_parts(col)
    lane = lax.broadcasted_iota(jnp.int32, (rows, 128), 1)
    extra[...] = jnp.where(
        lane == 0, hi, jnp.where(lane == 1, mid, jnp.where(lane == 2, low, 0.0))
    )
    value[...] = (
        parts[:, pl.ds(at, width)].astype(F4) + ra[:rows, :].astype(F4) + la[:rows, :].astype(F4)
    )

    def one(s, carry):
        at = pl.ds(pl.multiple_of(s * step, 8), step)
        to = pl.ds(pl.multiple_of(s * 2 * step, 16), 2 * step)
        v, e = value[at, :], extra[at, :]
        both = jnp.concatenate([v[:, :half], v[:, half:]], axis=0)
        out[to, :half] = both.astype(BF)
        out[to, half:] = jnp.concatenate([e, e], axis=0).astype(BF)
        return carry

    lax.fori_loop(0, n_sp, one, 0)


def grads_body(z, *refs, n, add, offsets):
    xs1, xs2, x4 = refs[:3]
    cb = refs[3 : n + 3]
    backs, act = refs[n + 3], refs[n + 4]
    refs = refs[n + 5 :]
    if add:
        old_h, gate, up, down, old, xbuf, cbuf, sems = refs
    else:
        out, xbuf, cbuf, sems = refs
    rows, width = x4.shape
    hid = act.shape[1]
    groups = []
    for k in range(n):
        groups.append([(cb[k], cbuf.at[pl.ds(k * rows, rows), :])])
    at = 0
    for x in (xs1, xs2, x4):
        groups[0].append((x, xbuf.at[pl.ds(at, x.shape[0]), :]))
        at += x.shape[0]
    if add:
        groups[0].append((old_h, old))

    def step(k, carry):
        at = pl.multiple_of(lax.rem(z[0] + offset_of(k, offsets, n), n) * width, width)
        mine = pl.ds(pl.multiple_of(k * rows, rows), rows)
        pair = dot(xbuf[mine, :], backs[...], 0, 0)
        dn = dot(act[...], cbuf[mine, :], 0, 0)
        if add:
            gate[pl.ds(at, width), :] = pair[:, :hid] + old[0, pl.ds(at, width), :].astype(F4)
            up[pl.ds(at, width), :] = pair[:, hid:] + old[1, pl.ds(at, width), :].astype(F4)
            for q in range(width // hid):
                lo = pl.multiple_of(at + q * hid, hid)
                down[:, pl.ds(lo, hid)] = dn[:, q * hid : (q + 1) * hid] + old[
                    2, pl.ds(lo, hid), :
                ].astype(F4)
        else:
            out[0, pl.ds(at, width), :] = pair[:, :hid].astype(BF)
            out[1, pl.ds(at, width), :] = pair[:, hid:].astype(BF)
            for q in range(width // hid):
                lo = pl.multiple_of(at + q * hid, hid)
                out[2, pl.ds(lo, hid), :] = dn[:, q * hid : (q + 1) * hid].astype(BF)
        return carry

    loaded(groups, sems, step)


def grads(z, xs, x4, cb, backs, act, old, offsets):
    rows, width = x4.shape
    n, hid = len(cb), act.shape[1]
    add = old is not None
    total = n * width
    args = [z, *xs, x4, *cb, backs, act] + ([old] if add else [])
    if add:
        out_shape = tuple(
            jax.ShapeDtypeStruct(t, F4) for t in ((total, hid), (total, hid), (hid, total))
        )
        out_specs = (VMEM,) * 3
    else:
        out_shape, out_specs = jax.ShapeDtypeStruct((3, total, hid), BF), VMEM
    return pl.pallas_call(
        lambda *r: grads_body(*r, n=n, add=add, offsets=offsets),
        out_shape=out_shape,
        in_specs=[SMEM] + [ANY] * (n + 3) + [VMEM] * 2 + ([ANY] if add else []),
        out_specs=out_specs,
        scratch_shapes=([pltpu.VMEM((3, total, hid), BF)] if add else [])
        + [
            pltpu.VMEM((n * rows, width), BF),
            pltpu.VMEM((n * rows, width), BF),
            pltpu.SemaphoreType.DMA((n + 4,)),
        ],
        compiler_params=BIG,
        cost_estimate=pl.CostEstimate(
            flops=8 * rows * total * 3 * hid, transcendentals=0, bytes_accessed=16 * 2**20
        ),
        name="grads_own" if add else "grads_other",
    )(*args)


def stack_body(*refs):
    out, at = refs[-1], 0
    for src in refs[:-1]:
        out[pl.ds(at, src.shape[0]), :] = src[...]
        at += src.shape[0]


def mixed_body(zc, mine, other, w_out, slope, out, *, n):
    width = mine.shape[2]
    out[...] = jnp.zeros(out.shape, F4)

    def step(k, carry):
        base = 2 * lax.rem(zc[0] + k, n)
        a = pl.multiple_of((base + zc[1]) * width, width)
        b = pl.multiple_of((base + 1 - zc[1]) * width, width)
        out[...] += dot(mine[k], w_out[:, pl.ds(a, width)], 1, 1) + dot(
            other[k], w_out[:, pl.ds(b, width)], 1, 1
        )
        return carry

    lax.fori_loop(0, n, step, 0)
    out[...] *= slope[...]


def outer_body(zc, mine, other, mixed_t, out, *, n):
    def step(k, carry):
        base = 2 * lax.rem(zc[0] + k, n)
        out[base + zc[1]] = dot(mixed_t[...], mine[k], 1, 0).astype(BF)
        out[base + 1 - zc[1]] = dot(mixed_t[...], other[k], 1, 0).astype(BF)
        return carry

    lax.fori_loop(0, n, step, 0)


def conv_body(back, rim, taps, value_in, gate_in, value_grad, gate_grad, padded):
    toks, n_taps = back.shape[0], taps.shape[0]
    padded[:toks, :] = back[...]
    padded[toks:, :] = rim[...]
    step = 128
    for at in range(0, toks, step):
        acc = jnp.zeros((step, back.shape[1]), F4)

        def one(tap, acc, at=at):
            lo = at + n_taps - 1 - tap
            return acc + taps[pl.ds(tap, 1), :] * padded[pl.ds(lo, step), :]

        acc = lax.fori_loop(0, n_taps, one, acc)
        sigma = jax.nn.sigmoid(gate_in[at : at + step, :].astype(F4))
        value = acc * sigma
        value_grad[at : at + step, :] = value.astype(BF)
        gate_grad[at : at + step, :] = (
            value * value_in[at : at + step, :].astype(F4) * (1.0 - sigma)
        ).astype(BF)


def per_device(
    upstream,
    stream,
    norm_gain,
    routes,
    route_weights,
    w_gate,
    w_up,
    w_down,
    value_in,
    gate_in,
    conv_pre,
    ln_gain,
    conv_taps,
    w_out,
):
    tok_rows, width_part = stream.shape
    n_sp = lax.axis_size("sp")
    n_z = lax.axis_size("z")
    n_tp = 2 * n_z
    z = lax.axis_index("z")
    core = lax.axis_index("c")
    model_width = width_part * n_tp
    channels = conv_pre.shape[1] * n_tp
    tap_count = conv_taps.shape[0]
    capacity = 3 * tok_rows // n_sp
    half_cap = capacity // 2
    experts = n_sp
    slot_count = experts * capacity
    rows = n_sp * half_cap
    wide = 2 * width_part

    zs = z.astype(jnp.int32).reshape(1)
    half = n_z // 2
    hid = w_gate.shape[2]

    picker, sent = pl.pallas_call(
        lambda *r: scatter_body(*r, experts=experts, capacity=capacity),
        out_shape=(
            jax.ShapeDtypeStruct((slot_count, tok_rows), BF),
            jax.ShapeDtypeStruct((2 * slot_count, width_part), BF),
        ),
        in_specs=[HBM] * 4,
        out_specs=(VMEM, VMEM),
        scratch_shapes=[
            pltpu.VMEM((2, tok_rows), jnp.int32),
            pltpu.VMEM((2, tok_rows), F4),
            pltpu.VMEM(upstream.shape, BF),
            pltpu.VMEM(stream.shape, BF),
            pltpu.SemaphoreType.DMA((4,)),
        ],
        compiler_params=BIG,
        name="scatter",
    )(routes.T, route_weights.T, upstream, stream)
    arrived = lax.all_to_all(
        sent.reshape(2 * experts, capacity, width_part), ("sp", "c"), 0, 0, tiled=True
    )
    x0, c0 = pl.pallas_call(
        lambda *r: unpack_body(*r, n_sp=n_sp),
        out_shape=(jax.ShapeDtypeStruct((rows, wide), BF),) * 2,
        in_specs=[VMEM],
        out_specs=(VMEM, VMEM),
        compiler_params=BIG,
        name="unpack",
    )(arrived.reshape(2 * slot_count, width_part))

    gu_own = jnp.concatenate([w_gate[0], w_up[0]], axis=1)
    weights = (gu_own, swap(gu_own), w_down[0], swap(w_down[0]))

    residual = stream.astype(F4)
    conv_vals = conv_pre.astype(F4)
    own_rows = x0.astype(F4)
    row_part = jnp.sum(own_rows * own_rows, axis=1)
    nothing = jnp.zeros_like(row_part)
    vector = jnp.concatenate(
        [
            jnp.sum(residual * residual, axis=1),
            jnp.sum(conv_vals, axis=1),
            jnp.sum(conv_vals * conv_vals, axis=1),
            jnp.where(core == 0, row_part, nothing),
            jnp.where(core == 0, nothing, row_part),
            norm_gain,
        ]
    )
    told = lax.all_to_all(
        jnp.broadcast_to(vector[None, None], (n_tp, 1, vector.size)), TP, 0, 0, tiled=True
    )[:, 0]
    cut = 3 * tok_rows + 2 * rows
    total = jnp.sum(told[:, :cut], axis=0)
    gains = told[:, cut:].reshape(n_z, wide)
    row_squares, conv_total, conv_squares = jnp.split(total[: 3 * tok_rows], 3)
    slot_squares = jnp.where(
        core == 0, total[3 * tok_rows : 3 * tok_rows + rows], total[3 * tok_rows + rows :]
    )
    inverse = lax.rsqrt(row_squares / model_width + EPSILON)[:, None]
    slot_inverse = lax.rsqrt(slot_squares / model_width + EPSILON)[:, None]

    xr, cl, cr, xl = [x0], [c0], [c0], [x0]
    for _ in range(half - 1):
        xr.append(right(xr[-1]))
        cl.append(left(cl[-1]))
        cr.append(right(cr[-1]))
        xl.append(left(xl[-1]))
    xf, cf = right(xr[-1]), left(cl[-1])
    offsets = (0, -1, 1, -2, 2, -3, 3, 4)
    xb, cb = [x0], [c0]
    for k in range(1, half):
        xb += [xr[k], xl[k]]
        cb += [cr[k], cl[k]]
    *sums, xs1 = project(
        zs, xb[:5], cb[:5], weights, gains, slot_inverse, offsets[:5], n_z, None
    )
    own, oth, back, xs2 = project(
        zs, xb[5:], cb[5:], weights, gains, slot_inverse, offsets[5:-1], n_z, sums
    )
    xs = (xs1, xs2)
    cb.append(cf)

    x4, b_own, b_oth, a_own, a_oth, along, ra, la = pl.pallas_call(
        lambda *r: finish_body(*r, n=n_z),
        out_shape=(
            jax.ShapeDtypeStruct((rows, wide), BF),
            jax.ShapeDtypeStruct((rows, 2 * hid), BF),
            jax.ShapeDtypeStruct((rows, 2 * hid), BF),
            jax.ShapeDtypeStruct((rows, hid), BF),
            jax.ShapeDtypeStruct((rows, hid), BF),
            jax.ShapeDtypeStruct((8, wide), F4),
            jax.ShapeDtypeStruct((rows // 2 + 16, wide), BF),
            jax.ShapeDtypeStruct((rows // 2, wide), BF),
        ),
        in_specs=[SMEM] + [VMEM] * 2 + [ANY] * 4 + [VMEM] * 5,
        out_specs=(ANY,) * 5 + (VMEM,) * 3,
        scratch_shapes=[
            pltpu.VMEM((rows, wide), BF),
            pltpu.VMEM((rows, 2 * hid), BF),
            pltpu.VMEM((rows, 2 * hid), BF),
            pltpu.VMEM((rows, hid), BF),
            pltpu.VMEM((rows, hid), BF),
            pltpu.VMEM((wide, 2 * hid), BF),
            pltpu.VMEM((wide, 2 * hid), BF),
            pltpu.VMEM((hid, wide), BF),
            pltpu.VMEM((hid, wide), BF),
            pltpu.SemaphoreType.DMA((5,)),
        ],
        compiler_params=BIG,
        name="finish",
    )(zs, xf, cf, *weights, gains, slot_inverse, own, oth, back)

    ra, la = right(ra), left(la)
    parts = pl.pallas_call(
        lambda *r: parts_body(*r, n=n_z),
        out_shape=jax.ShapeDtypeStruct((rows, model_width), BF),
        in_specs=[VMEM] * 2 + [ANY] * 2,
        out_specs=VMEM,
        scratch_shapes=[
            pltpu.VMEM((model_width, 2 * hid), BF),
            pltpu.VMEM((model_width, 2 * hid), BF),
            pltpu.SemaphoreType.DMA((2 * n_z,)),
        ],
        compiler_params=BIG,
        name="parts",
    )(b_own, b_oth, *weights[:2])
    message = jax.ShapeDtypeStruct((rows + 16, wide), BF)
    for k in range(half - 1, 0, -1):
        ra, la = pl.pallas_call(
            lambda *r, k=k: hop_body(*r, k=k, n=n_z, first=k == half - 1),
            out_shape=(message, message),
            in_specs=[SMEM] + [VMEM] * 4,
            out_specs=(VMEM, VMEM),
            compiler_params=BIG,
            name="hop",
        )(zs, parts, along, ra, la)
        ra, la = right(ra), left(la)
        if k == 2:
            others = grads(zs, xs, x4, cb, b_oth, a_oth, None, offsets)
            ra, la, others = lax.optimization_barrier((ra, la, others))
    sent_back = pl.pallas_call(
        lambda *r: pack_body(*r, n_sp=n_sp),
        out_shape=jax.ShapeDtypeStruct((slot_count, width_part + 128), BF),
        in_specs=[SMEM] + [VMEM] * 4,
        out_specs=VMEM,
        scratch_shapes=[pltpu.VMEM((rows, wide), F4), pltpu.VMEM((rows, 128), F4)],
        compiler_params=BIG,
        name="pack",
    )(zs, parts, along, ra, la)
    sent_back, others = lax.optimization_barrier((sent_back, others))
    others = swap(others)
    returned = lax.all_to_all(
        sent_back.reshape(2 * n_sp, half_cap, width_part + 128), ("sp", "c"), 0, 0, tiled=True
    ).reshape(slot_count, width_part + 128)

    token_back = dot(picker, returned, 0, 0)
    inner = jnp.sum(token_back[:, width_part : width_part + 3], axis=1, keepdims=True)
    gained = norm_gain[None, :] * token_back[:, :width_part]
    norm_back = inverse * gained - residual * inverse**2 * (inner / model_width)
    stream_grad = (upstream.astype(F4) + norm_back).astype(BF)

    p1, m1, p2, m2 = (hops(stream_grad, d) for d in (1, -1, 2, -2))
    p3, m3 = hops(p1, 2), hops(m1, -2)
    far = hops(p2, 2)
    mine8 = pl.pallas_call(
        stack_body,
        out_shape=jax.ShapeDtypeStruct((n_z * tok_rows, width_part), BF),
        in_specs=[VMEM] * 8,
        out_specs=VMEM,
        compiler_params=BIG,
        name="stack",
    )(stream_grad, m1, m2, m3, far, p3, p2, p1).reshape(n_z, tok_rows, width_part)
    other8 = swap(mine8)

    mean_val = (conv_total / channels)[:, None]
    variance = (conv_squares / channels)[:, None] - mean_val * mean_val
    inv_std = lax.rsqrt(variance + EPSILON)
    centred = (conv_vals - mean_val) * inv_std
    scaled = centred * ln_gain[None, :]
    mixed_out = jax.nn.silu(scaled).astype(BF)

    zc = jnp.stack([z, core]).astype(jnp.int32)
    slope = silu_slope(scaled) * ln_gain[None, :]
    norm_in = pl.pallas_call(
        lambda *r: mixed_body(*r, n=n_z),
        out_shape=jax.ShapeDtypeStruct(conv_pre.shape, F4),
        in_specs=[SMEM] + [VMEM] * 4,
        out_specs=VMEM,
        compiler_params=BIG,
        name="mixed",
    )(zc, mine8, other8, w_out, slope)
    out_parts = pl.pallas_call(
        lambda *r: outer_body(*r, n=n_z),
        out_shape=jax.ShapeDtypeStruct((n_sp, conv_pre.shape[1], width_part), BF),
        in_specs=[SMEM] + [VMEM] * 3,
        out_specs=VMEM,
        compiler_params=BIG,
        name="outer",
    )(zc, mine8, other8, mixed_out.T)
    norm_total, norm_cross = in_one((jnp.sum(norm_in, axis=1), jnp.sum(norm_in * centred, axis=1)))
    conv_back = inv_std * (
        norm_in - (norm_total / channels)[:, None] - centred * (norm_cross / channels)[:, None]
    )
    next_rim = lax.ppermute(conv_back[:32], "sp", [(i + 1, i) for i in range(n_sp - 1)])
    out_blocks = lax.all_to_all(out_parts, "sp", 0, 0, tiled=True)
    grad_gate, grad_up, grad_down = grads(zs, xs, x4, cb, b_own, a_own, others, offsets)
    conv_back, grad_gate, grad_up, grad_down = lax.optimization_barrier(
        (conv_back, grad_gate, grad_up, grad_down)
    )
    value_grad, gate_grad = pl.pallas_call(
        conv_body,
        out_shape=(jax.ShapeDtypeStruct(value_in.shape, BF),) * 2,
        in_specs=[VMEM] * 5,
        out_specs=(VMEM, VMEM),
        scratch_shapes=[pltpu.VMEM((tok_rows + 32, conv_pre.shape[1]), F4)],
        name="conv",
    )(conv_back, next_rim, conv_taps, value_in, gate_in)
    out_blocks, value_grad = lax.optimization_barrier((out_blocks, value_grad))
    grad_out = jnp.sum(out_blocks.astype(F4), axis=0)
    return (grad_gate[None], grad_up[None], grad_down[None], grad_out, value_grad, gate_grad)


def solution(mesh):
    n_sp, n_tp = mesh.devices.shape
    split = Mesh(mesh.devices.reshape(n_sp, n_tp // 2, 2), ("sp", "z", "c"))
    return jax.shard_map(
        per_device,
        mesh=split,
        in_specs=(
            P("sp", TP),
            P("sp", TP),
            P(TP),
            P("sp", None),
            P("sp", None),
            P("sp", None, TP),
            P("sp", None, TP),
            P("sp", TP, None),
            P("sp", TP),
            P("sp", TP),
            P("sp", TP),
            P(TP),
            P(None, TP),
            P(TP, None),
        ),
        out_specs=(
            P("sp", None, TP),
            P("sp", None, TP),
            P("sp", TP, None),
            P(TP, "sp"),
            P("sp", TP),
            P("sp", TP),
        ),
        check_vma=False,
    )
```

profile of v0, /device:TPU:1, one launch (start us, length us, event | category | flops | bytes accessed | tf_op | source)
XLA Modules:
  0.0 234.3 jit_solution(9392060586761435895)
XLA Ops:
  0.6 3.3 %collective-permute-start.9 = (bf16[128,4096]{1,0:T(8,128)(2,1)}, bf16[128,4096]{1,0:T(8,128)(2,1)}, u32[]{:S(2)}, u32[]{:S(2)}) collective-permute-start(bf16[128,4096]{1,0:T(8,128)(2,1)} %bitcast.25), channel_id=1, source_target_pairs={{0,1},{1,0},{2,3},{3,2},{4,5},{5,4},{6,7},{7,6},{8,9},{9,8},{10,11... | collective-permute-start | bytes 3145736 | tf_op jit(solution)/shard_map/ppermute | solution.py:47
  7.1 3.4 %scatter.1 = (bf16[768,256]{1,0:T(8,128)(2,1)S(1)}, bf16[1536,256]{1,0:T(8,128)(2,1)}) custom-call(s32[2,256]{1,0:T(2,128)S(1)} %bitcast.29, f32[2,256]{1,0:T(2,128)S(1)} %bitcast.30, bf16[256,256]{1,0:T(8,128)(2,1)S(1)} %copy-done.4, bf16[256,256]{1,0:T(8,128)(2,1)S(1)} %copy-done.1), custom_call_target="tpu_custom_call" | custom-call | tf_op jit(solution)/shard_map/scatter/pallas_call | solution.py:556
  11.3 5.5 %all-to-all-start = ((bf16[32,48,256]{2,1,0:T(8,128)(2,1)}), bf16[32,48,256]{2,1,0:T(8,128)(2,1)}, u32[]{:S(2)}, u32[]{:S(2)}) async-start(bf16[32,48,256]{2,1,0:T(8,128)(2,1)} %bitcast.2), calls=%async_computation | async-start | bytes 1572864 | tf_op jit(solution)/shard_map/all_to_all | solution.py:574
  18.7 12.4 %all-to-all-done = bf16[32,48,256]{2,1,0:T(8,128)(2,1)} async-done(((bf16[32,48,256]{2,1,0:T(8,128)(2,1)}), bf16[32,48,256]{2,1,0:T(8,128)(2,1)}, u32[]{:S(2)}, u32[]{:S(2)}) %all-to-all-start) | async-done | bytes 786464 | tf_op jit(solution)/shard_map/all_to_all | solution.py:574
  34.7 3.9 %collective-permute-start.4 = (bf16[384,512]{1,0:T(8,128)(2,1)}, bf16[384,512]{1,0:T(8,128)(2,1)}, u32[]{:S(2)}, u32[]{:S(2)}) collective-permute-start(bf16[384,512]{1,0:T(8,128)(2,1)} %get-tuple-element.51.r_6_.r_4_), channel_id=1, source_target_pairs={{0,14},{2,0},{4,2},{6,4},{8,6},{10,8},{12,10},{14,12},{1,15},{3,1}... | collective-permute-start | bytes 1179656 | tf_op jit(solution)/shard_map/ppermute | solution.py:38
  42.2 5.5 %collective-permute-done.r_2_ = bf16[384,512]{1,0:T(8,128)(2,1)} collective-permute-done((bf16[384,512]{1,0:T(8,128)(2,1)S(1)}, bf16[384,512]{1,0:T(8,128)(2,1)}, u32[]{:S(2)}, u32[]{:S(2)}) %collective-permute-start) | collective-permute-done | bytes 393248 | tf_op jit(solution)/shard_map/ppermute | solution.py:33
  47.7 2.7 %collective-permute-start.5 = (bf16[384,512]{1,0:T(8,128)(2,1)}, bf16[384,512]{1,0:T(8,128)(2,1)}, u32[]{:S(2)}, u32[]{:S(2)}) collective-permute-start(bf16[384,512]{1,0:T(8,128)(2,1)} %collective-permute-done.4.r_8_.r_6_), channel_id=1, source_target_pairs={{0,14},{2,0},{4,2},{6,4},{8,6},{10,8},{12,10},{14,12},{1,15},{3,1}... | collective-permute-start | bytes 1179656 | tf_op jit(solution)/shard_map/ppermute | solution.py:38
  50.5 4.7 %collective-permute-done.10.r_3_ = bf16[384,512]{1,0:T(8,128)(2,1)} collective-permute-done((bf16[384,512]{1,0:T(8,128)(2,1)S(1)}, bf16[384,512]{1,0:T(8,128)(2,1)}, u32[]{:S(2)}, u32[]{:S(2)}) %collective-permute-start.10) | collective-permute-done | bytes 393248 | tf_op jit(solution)/shard_map/ppermute | solution.py:38
  55.2 3.5 %collective-permute-start.11 = (bf16[384,512]{1,0:T(8,128)(2,1)}, bf16[384,512]{1,0:T(8,128)(2,1)}, u32[]{:S(2)}, u32[]{:S(2)}) collective-permute-start(bf16[384,512]{1,0:T(8,128)(2,1)} %collective-permute-done.10.r_3_), channel_id=1, source_target_pairs={{0,14},{2,0},{4,2},{6,4},{8,6},{10,8},{12,10},{14,12},{1,15},{3,1}... | collective-permute-start | bytes 1179656 | tf_op jit(solution)/shard_map/ppermute | solution.py:38
  58.7 5.8 %collective-permute-done.1.r_4_ = bf16[384,512]{1,0:T(8,128)(2,1)} collective-permute-done((bf16[384,512]{1,0:T(8,128)(2,1)}, bf16[384,512]{1,0:T(8,128)(2,1)}, u32[]{:S(2)}, u32[]{:S(2)}) %collective-permute-start.1) | collective-permute-done | bytes 393248 | tf_op jit(solution)/shard_map/ppermute | solution.py:33
  64.5 2.7 %collective-permute-start.6 = (bf16[384,512]{1,0:T(8,128)(2,1)}, bf16[384,512]{1,0:T(8,128)(2,1)}, u32[]{:S(2)}, u32[]{:S(2)}) collective-permute-start(bf16[384,512]{1,0:T(8,128)(2,1)} %collective-permute-done.5.r_10_.r_8_), channel_id=1, source_target_pairs={{0,14},{2,0},{4,2},{6,4},{8,6},{10,8},{12,10},{14,12},{1,15},{3,1}... | collective-permute-start | bytes 1179656 | tf_op jit(solution)/shard_map/ppermute | solution.py:38
  67.9 8.4 %all-to-all-start.1 = ((f32[16,1,1792]{2,1,0:T(1,128)}), f32[16,1,1792]{2,1,0:T(1,128)}, u32[]{:S(2)}, u32[]{:S(2)}) async-start(f32[16,1,1792]{2,1,0:T(1,128)} %broadcast_in_dim.15), calls=%async_computation.1 | async-start | bytes 229376 | tf_op jit(solution)/shard_map/all_to_all | solution.py:604
  81.5 3.6 %collective-permute-start.7 = (bf16[384,512]{1,0:T(8,128)(2,1)}, bf16[384,512]{1,0:T(8,128)(2,1)}, u32[]{:S(2)}, u32[]{:S(2)}) collective-permute-start(bf16[384,512]{1,0:T(8,128)(2,1)} %collective-permute-done.6.r_4_.r_10_), channel_id=1, source_target_pairs={{0,14},{2,0},{4,2},{6,4},{8,6},{10,8},{12,10},{14,12},{1,15},{3,1}... | collective-permute-start | bytes 1179656 | tf_op jit(solution)/shard_map/ppermute | solution.py:38
  90.7 6.7 %project.2 = (f32[384,256]{1,0:T(8,128)S(1)}, f32[384,256]{1,0:T(8,128)S(1)}, f32[384,256]{1,0:T(8,128)S(1)}, bf16[1920,512]{1,0:T(8,128)(2,1)S(1)}) custom-call(s32[1]{0:T(128)} %bitcast.4.r_0_, bf16[384,512]{1,0:T(8,128)(2,1)S(1)} %get-tuple-element.49.r_1_, bf16[384,512]{1,0:T(8,128)(2,1)} %collective-permute-done.r_2_, ...), custom_call_target="tpu_custom_call" | custom-call | tf_op jit(solution)/shard_map/project/pallas_call | solution.py:210
  97.5 3.7 %project.3 = (f32[384,256]{1,0:T(8,128)S(1)}, f32[384,256]{1,0:T(8,128)S(1)}, f32[384,256]{1,0:T(8,128)S(1)}, bf16[768,512]{1,0:T(8,128)(2,1)S(1)}) custom-call(s32[1]{0:T(128)} %bitcast.4.r_0_, bf16[384,512]{1,0:T(8,128)(2,1)} %collective-permute-done.2.r_1_, bf16[384,512]{1,0:T(8,128)(2,1)} %collective-permute-done.12.r_2_, ...), custom_call_target="tpu_custom_call" | custom-call | tf_op jit(solution)/shard_map/project/pallas_call | solution.py:210
  101.2 4.5 %finish.1 = (bf16[384,512]{1,0:T(8,128)(2,1)S(1)}, bf16[384,256]{1,0:T(8,128)(2,1)S(1)}, bf16[384,256]{1,0:T(8,128)(2,1)S(1)}, bf16[384,128]{1,0:T(8,128)(2,1)S(...) custom-call(s32[1]{0:T(128)} %bitcast.4.r_0_, ...), custom_call_target="tpu_custom_call" | custom-call | tf_op jit(solution)/shard_map/finish/pallas_call | solution.py:638
  105.8 3.4 %collective-permute-start.16 = (bf16[208,512]{1,0:T(8,128)(2,1)S(1)}, bf16[208,512]{1,0:T(8,128)(2,1)S(1)}, u32[]{:S(2)}, u32[]{:S(2)}) collective-permute-start(bf16[208,512]{1,0:T(8,128)(2,1)S(1)} %get-tuple-element.61), channel_id=1, source_target_pairs={{0,2},{2,4},{4,6},{6,8},{8,10},{10,12},{12,14},{14,0},{1,3},{3,5},... | collective-permute-start | bytes 638984 | tf_op jit(solution)/shard_map/ppermute | solution.py:33
  109.2 4.3 %parts.1.r_1_ = bf16[384,4096]{1,0:T(8,128)(2,1)S(1)} custom-call(bf16[384,256]{1,0:T(8,128)(2,1)S(1)} %get-tuple-element.58.r_0_.r_12_, bf16[384,256]{1,0:T(8,128)(2,1)S(1)} %get-tuple-element.59.r_1_.r_12_, bf16[4096,256]{1,0:T(8,128)(2,1)S(1)} %pad_maximum_fusion.r_11_.r_5_.r_3_.r_2_, bf16[4096,256]{1,0:T(8,128)(2,1)} %collective-permute-done.8.r_12_.r_6_.r_4_.r_3_), custom_call_target="tpu_custom_call" | custom-call | tf_op jit(solution)/shard_map/parts/pallas_call | solution.py:669
  118.2 8.3 %collective-permute-done.18.r_3_ = bf16[400,512]{1,0:T(8,128)(2,1)S(1)} collective-permute-done((bf16[400,512]{1,0:T(8,128)(2,1)S(1)}, bf16[400,512]{1,0:T(8,128)(2,1)S(1)}, u32[]{:S(2)}, u32[]{:S(2)}) %collective-permute-start.18) | collective-permute-done | bytes 409632 | tf_op jit(solution)/shard_map/ppermute | solution.py:33
  129.4 5.7 %grads_other.1 = bf16[3,4096,128]{2,1,0:T(8,128)(2,1)S(1)} custom-call(s32[1]{0:T(128)} %bitcast.4.r_0_, bf16[1920,512]{1,0:T(8,128)(2,1)S(1)} %get-tuple-element.67.r_1_, bf16[768,512]{1,0:T(8,128)(2,1)S(1)} %get-tuple-element.68.r_2_, bf16[384,512]{1,0:T(8,128)(2,1)S(1)} %get-tuple-element.69.r_3_, bf16[384,512]{1,0:T(8,128)(2,1)} %get-tuple-element.51.r_6_.r_4_, ...), custom_call_target="tpu_custom_call" | custom-call | flops 4831838208 | bytes 16777216 | tf_op jit(solution)/shard_map/grads_other/pallas_call | solution.py:446
  139.9 6.6 %collective-permute-done.22.r_3_ = bf16[400,512]{1,0:T(8,128)(2,1)S(1)} collective-permute-done((bf16[400,512]{1,0:T(8,128)(2,1)S(1)}, bf16[400,512]{1,0:T(8,128)(2,1)S(1)}, u32[]{:S(2)}, u32[]{:S(2)}) %collective-permute-start.22) | collective-permute-done | bytes 409632 | tf_op jit(solution)/shard_map/ppermute | solution.py:33
  147.7 7.7 %all-to-all-start.2 = ((bf16[32,24,384]{2,1,0:T(8,128)(2,1)}), bf16[32,24,384]{2,1,0:T(8,128)(2,1)S(1)}, u32[]{:S(2)}, u32[]{:S(2)}) async-start(bf16[32,24,384]{2,1,0:T(8,128)(2,1)} %bitcast.9), calls=%async_computation.2 | async-start | bytes 1179648 | tf_op jit(solution)/shard_map/all_to_all | solution.py:707
  156.7 11.0 %all-to-all-done.2 = bf16[32,24,384]{2,1,0:T(8,128)(2,1)S(1)} async-done(((bf16[32,24,384]{2,1,0:T(8,128)(2,1)}), bf16[32,24,384]{2,1,0:T(8,128)(2,1)S(1)}, u32[]{:S(2)}, u32[]{:S(2)}) %all-to-all-start.2) | async-done | bytes 589856 | tf_op jit(solution)/shard_map/all_to_all | solution.py:707
  174.4 5.3 %collective-permute-done.27.refs_6_ = bf16[256,256]{1,0:T(8,128)(2,1)S(1)} collective-permute-done((bf16[256,256]{1,0:T(8,128)(2,1)S(1)}, bf16[256,256]{1,0:T(8,128)(2,1)S(1)}, u32[]{:S(2)}, u32[]{:S(2)}) %collective-permute-start.27) | collective-permute-done | bytes 131104 | tf_op jit(solution)/shard_map/ppermute | solution.py:43
  179.7 3.6 %collective-permute-start.26 = (bf16[256,256]{1,0:T(8,128)(2,1)S(1)}, bf16[256,256]{1,0:T(8,128)(2,1)S(1)}, u32[]{:S(2)}, u32[]{:S(2)}) collective-permute-start(bf16[256,256]{1,0:T(8,128)(2,1)S(1)} %collective-permute-done.24.refs_1_), channel_id=1, source_target_pairs={{0,12},{2,14},{4,0},{6,2},{8,4},{10,6},{12,8},{14,10},{1,13},{3,15... | collective-permute-start | bytes 393224 | tf_op jit(solution)/shard_map/ppermute | solution.py:43
  184.9 5.3 %collective-permute-done.28.refs_4_ = bf16[256,256]{1,0:T(8,128)(2,1)S(1)} collective-permute-done((bf16[256,256]{1,0:T(8,128)(2,1)S(1)}, bf16[256,256]{1,0:T(8,128)(2,1)S(1)}, u32[]{:S(2)}, u32[]{:S(2)}) %collective-permute-start.28) | collective-permute-done | bytes 131104 | tf_op jit(solution)/shard_map/ppermute | solution.py:43
  190.2 3.6 %collective-permute-start.31 = (bf16[8,256,256]{2,1,0:T(8,128)(2,1)S(1)}, bf16[8,256,256]{2,1,0:T(8,128)(2,1)S(1)}, u32[]{:S(2)}, u32[]{:S(2)}) collective-permute-start(bf16[8,256,256]{2,1,0:T(8,128)(2,1)S(1)} %bitcast.22), channel_id=1, source_target_pairs={{0,1},{1,0},{2,3},{3,2},{4,5},{5,4},{6,7},{7,6},{8,9},{9,8},{10,11... | collective-permute-start | bytes 3145736 | tf_op jit(solution)/shard_map/ppermute | solution.py:47
  199.5 4.1 %all-to-all-start.3 = ((f32[16,1,512]{2,1,0:T(1,128)}), f32[16,1,512]{2,1,0:T(1,128)S(1)}, u32[]{:S(2)}, u32[]{:S(2)}) async-start(f32[16,1,512]{2,1,0:T(1,128)} %broadcast_in_dim.17), calls=%async_computation.3 | async-start | bytes 65536 | tf_op jit(solution)/shard_map/all_to_all | solution.py:16
  203.8 3.1 %outer.1 = bf16[16,128,256]{2,1,0:T(8,128)(2,1)} custom-call(s32[2]{0:T(128)S(1)} %pad_add_fusion.r_0_, bf16[8,256,256]{2,1,0:T(8,128)(2,1)S(1)} %bitcast.24, bf16[8,256,256]{2,1,0:T(8,128)(2,1)S(1)} %collective-permute-done.31.r_2_, bf16[128,256]{1,0:T(8,128)(2,1)S(1)} %copy.37.r_3_), custom_call_target="tpu_custom_call" | custom-call | tf_op jit(solution)/shard_map/outer/pallas_call | solution.py:747
  206.9 4.1 %all-to-all-done.3 = f32[16,1,512]{2,1,0:T(1,128)S(1)} async-done(((f32[16,1,512]{2,1,0:T(1,128)}), f32[16,1,512]{2,1,0:T(1,128)S(1)}, u32[]{:S(2)}, u32[]{:S(2)}) %all-to-all-start.3) | async-done | bytes 32800 | tf_op jit(solution)/shard_map/all_to_all | solution.py:16
  211.1 4.3 %all-to-all-start.4 = ((bf16[16,128,256]{2,1,0:T(8,128)(2,1)}), bf16[16,128,256]{2,1,0:T(8,128)(2,1)}, u32[]{:S(2)}, u32[]{:S(2)}) async-start(bf16[16,128,256]{2,1,0:T(8,128)(2,1)} %outer.1), calls=%async_computation.4 | async-start | bytes 2097152 | tf_op jit(solution)/shard_map/all_to_all | solution.py:760
  218.0 9.4 %grads_own.1 = (f32[4096,128]{1,0:T(8,128)}, f32[4096,128]{1,0:T(8,128)}, f32[128,4096]{1,0:T(8,128)}) custom-call(s32[1]{0:T(128)} %bitcast.4.r_0_, bf16[1920,512]{1,0:T(8,128)(2,1)S(1)} %copy-done.12, bf16[768,512]{1,0:T(8,128)(2,1)S(1)} %copy-done.14, bf16[384,512]{1,0:T(8,128)(2,1)S(1)} %copy-done.16, bf16[384,512]{1,0:T(8,128)(2,1)} %get-tuple-element.51.r_6_.r_4_, ...), custom_call_target="tpu_custom_call" | custom-call | flops 4831838208 | bytes 16777216 | tf_op jit(solution)/shard_map/grads_own/pallas_call | solution.py:446
  (152 shorter events, 62.7 us)
Async XLA Ops:
  0.6 41.6 %collective-permute-start.9 = (bf16[128,4096]{1,0:T(8,128)(2,1)}, bf16[128,4096]{1,0:T(8,128)(2,1)}, u32[]{:S(2)}, u32[]{:S(2)}) collective-permute-start(bf16[128,4096]{1,0:T(8,128)(2,1)} %bitcast.25), channel_id=1, source_target_pairs={{0,1},{1,0},{2,3},{3,2},{4,5},{5,4},{6,7},{7,6},{8,9},{9,8},{10,11... | collective-permute-start | bytes 3145736 | tf_op jit(solution)/shard_map/ppermute | solution.py:47
  11.3 19.8 %all-to-all-start = ((bf16[32,48,256]{2,1,0:T(8,128)(2,1)}), bf16[32,48,256]{2,1,0:T(8,128)(2,1)}, u32[]{:S(2)}, u32[]{:S(2)}) async-start(bf16[32,48,256]{2,1,0:T(8,128)(2,1)} %bitcast.2), calls=%async_computation | async-start | bytes 1572864 | tf_op jit(solution)/shard_map/all_to_all | solution.py:574
  18.3 72.0 %collective-permute-start.8 = (bf16[4096,256]{1,0:T(8,128)(2,1)S(1)}, bf16[4096,256]{1,0:T(8,128)(2,1)}, u32[]{:S(2)}, u32[]{:S(2)}) collective-permute-start(bf16[4096,256]{1,0:T(8,128)(2,1)S(1)} %pad_maximum_fusion.r_11_.r_5_.r_3_.r_2_), channel_id=1, source_target_pairs={{0,1},{1,0},{2,3},{3,2},{4,5},{5,4},{6,7},{7,6},{8,9},{9,8},{10,11... | collective-permute-start | bytes 6291464 | tf_op jit(solution)/shard_map/ppermute | solution.py:47
  33.0 14.7 %collective-permute-start = (bf16[384,512]{1,0:T(8,128)(2,1)S(1)}, bf16[384,512]{1,0:T(8,128)(2,1)}, u32[]{:S(2)}, u32[]{:S(2)}) collective-permute-start(bf16[384,512]{1,0:T(8,128)(2,1)S(1)} %get-tuple-element.49.r_1_), channel_id=1, source_target_pairs={{0,2},{2,4},{4,6},{6,8},{8,10},{10,12},{12,14},{14,0},{1,3},{3,5},... | collective-permute-start | bytes 1179656 | tf_op jit(solution)/shard_map/ppermute | solution.py:33
  34.7 13.0 %collective-permute-start.4 = (bf16[384,512]{1,0:T(8,128)(2,1)}, bf16[384,512]{1,0:T(8,128)(2,1)}, u32[]{:S(2)}, u32[]{:S(2)}) collective-permute-start(bf16[384,512]{1,0:T(8,128)(2,1)} %get-tuple-element.51.r_6_.r_4_), channel_id=1, source_target_pairs={{0,14},{2,0},{4,2},{6,4},{8,6},{10,8},{12,10},{14,12},{1,15},{3,1}... | collective-permute-start | bytes 1179656 | tf_op jit(solution)/shard_map/ppermute | solution.py:38
  40.6 14.6 %collective-permute-start.10 = (bf16[384,512]{1,0:T(8,128)(2,1)S(1)}, bf16[384,512]{1,0:T(8,128)(2,1)}, u32[]{:S(2)}, u32[]{:S(2)}) collective-permute-start(bf16[384,512]{1,0:T(8,128)(2,1)S(1)} %get-tuple-element.49.r_1_), channel_id=1, source_target_pairs={{0,14},{2,0},{4,2},{6,4},{8,6},{10,8},{12,10},{14,12},{1,15},{3,1}... | collective-permute-start | bytes 1179656 | tf_op jit(solution)/shard_map/ppermute | solution.py:38
  42.2 16.5 %collective-permute-start.13 = (bf16[384,512]{1,0:T(8,128)(2,1)}, bf16[384,512]{1,0:T(8,128)(2,1)}, u32[]{:S(2)}, u32[]{:S(2)}) collective-permute-start(bf16[384,512]{1,0:T(8,128)(2,1)} %get-tuple-element.51.r_6_.r_4_), channel_id=1, source_target_pairs={{0,2},{2,4},{4,6},{6,8},{8,10},{10,12},{12,14},{14,0},{1,3},{3,5},... | collective-permute-start | bytes 1179656 | tf_op jit(solution)/shard_map/ppermute | solution.py:33
  47.7 16.9 %collective-permute-start.1 = (bf16[384,512]{1,0:T(8,128)(2,1)}, bf16[384,512]{1,0:T(8,128)(2,1)}, u32[]{:S(2)}, u32[]{:S(2)}) collective-permute-start(bf16[384,512]{1,0:T(8,128)(2,1)} %collective-permute-done.r_2_), channel_id=1, source_target_pairs={{0,2},{2,4},{4,6},{6,8},{8,10},{10,12},{12,14},{14,0},{1,3},{3,5},... | collective-permute-start | bytes 1179656 | tf_op jit(solution)/shard_map/ppermute | solution.py:33
  47.7 16.9 %collective-permute-start.5 = (bf16[384,512]{1,0:T(8,128)(2,1)}, bf16[384,512]{1,0:T(8,128)(2,1)}, u32[]{:S(2)}, u32[]{:S(2)}) collective-permute-start(bf16[384,512]{1,0:T(8,128)(2,1)} %collective-permute-done.4.r_8_.r_6_), channel_id=1, source_target_pairs={{0,14},{2,0},{4,2},{6,4},{8,6},{10,8},{12,10},{14,12},{1,15},{3,1}... | collective-permute-start | bytes 1179656 | tf_op jit(solution)/shard_map/ppermute | solution.py:38
  55.2 21.2 %collective-permute-start.11 = (bf16[384,512]{1,0:T(8,128)(2,1)}, bf16[384,512]{1,0:T(8,128)(2,1)}, u32[]{:S(2)}, u32[]{:S(2)}) collective-permute-start(bf16[384,512]{1,0:T(8,128)(2,1)} %collective-permute-done.10.r_3_), channel_id=1, source_target_pairs={{0,14},{2,0},{4,2},{6,4},{8,6},{10,8},{12,10},{14,12},{1,15},{3,1}... | collective-permute-start | bytes 1179656 | tf_op jit(solution)/shard_map/ppermute | solution.py:38
  58.7 20.3 %collective-permute-start.14 = (bf16[384,512]{1,0:T(8,128)(2,1)}, bf16[384,512]{1,0:T(8,128)(2,1)}, u32[]{:S(2)}, u32[]{:S(2)}) collective-permute-start(bf16[384,512]{1,0:T(8,128)(2,1)} %collective-permute-done.13.r_7_.r_5_), channel_id=1, source_target_pairs={{0,2},{2,4},{4,6},{6,8},{8,10},{10,12},{12,14},{14,0},{1,3},{3,5},... | collective-permute-start | bytes 1179656 | tf_op jit(solution)/shard_map/ppermute | solution.py:33
  64.5 16.7 %collective-permute-start.2 = (bf16[384,512]{1,0:T(8,128)(2,1)}, bf16[384,512]{1,0:T(8,128)(2,1)}, u32[]{:S(2)}, u32[]{:S(2)}) collective-permute-start(bf16[384,512]{1,0:T(8,128)(2,1)} %collective-permute-done.1.r_4_), channel_id=1, source_target_pairs={{0,2},{2,4},{4,6},{6,8},{8,10},{10,12},{12,14},{14,0},{1,3},{3,5},... | collective-permute-start | bytes 1179656 | tf_op jit(solution)/shard_map/ppermute | solution.py:33
  64.5 17.0 %collective-permute-start.6 = (bf16[384,512]{1,0:T(8,128)(2,1)}, bf16[384,512]{1,0:T(8,128)(2,1)}, u32[]{:S(2)}, u32[]{:S(2)}) collective-permute-start(bf16[384,512]{1,0:T(8,128)(2,1)} %collective-permute-done.5.r_10_.r_8_), channel_id=1, source_target_pairs={{0,14},{2,0},{4,2},{6,4},{8,6},{10,8},{12,10},{14,12},{1,15},{3,1}... | collective-permute-start | bytes 1179656 | tf_op jit(solution)/shard_map/ppermute | solution.py:38
  67.9 18.4 %all-to-all-start.1 = ((f32[16,1,1792]{2,1,0:T(1,128)}), f32[16,1,1792]{2,1,0:T(1,128)}, u32[]{:S(2)}, u32[]{:S(2)}) async-start(f32[16,1,1792]{2,1,0:T(1,128)} %broadcast_in_dim.15), calls=%async_computation.1 | async-start | bytes 229376 | tf_op jit(solution)/shard_map/all_to_all | solution.py:604
  76.4 21.1 %collective-permute-start.12 = (bf16[384,512]{1,0:T(8,128)(2,1)}, bf16[384,512]{1,0:T(8,128)(2,1)}, u32[]{:S(2)}, u32[]{:S(2)}) collective-permute-start(bf16[384,512]{1,0:T(8,128)(2,1)} %collective-permute-done.11.r_5_), channel_id=1, source_target_pairs={{0,14},{2,0},{4,2},{6,4},{8,6},{10,8},{12,10},{14,12},{1,15},{3,1}... | collective-permute-start | bytes 1179656 | tf_op jit(solution)/shard_map/ppermute | solution.py:38
  79.0 18.5 %collective-permute-start.15 = (bf16[384,512]{1,0:T(8,128)(2,1)}, bf16[384,512]{1,0:T(8,128)(2,1)}, u32[]{:S(2)}, u32[]{:S(2)}) collective-permute-start(bf16[384,512]{1,0:T(8,128)(2,1)} %collective-permute-done.14.r_9_.r_7_), channel_id=1, source_target_pairs={{0,2},{2,4},{4,6},{6,8},{8,10},{10,12},{12,14},{14,0},{1,3},{3,5},... | collective-permute-start | bytes 1179656 | tf_op jit(solution)/shard_map/ppermute | solution.py:33
  81.3 19.9 %collective-permute-start.3 = (bf16[384,512]{1,0:T(8,128)(2,1)}, bf16[384,512]{1,0:T(8,128)(2,1)}, u32[]{:S(2)}, u32[]{:S(2)}) collective-permute-start(bf16[384,512]{1,0:T(8,128)(2,1)} %collective-permute-done.2.r_1_), channel_id=1, source_target_pairs={{0,2},{2,4},{4,6},{6,8},{8,10},{10,12},{12,14},{14,0},{1,3},{3,5},... | collective-permute-start | bytes 1179656 | tf_op jit(solution)/shard_map/ppermute | solution.py:33
  81.5 19.7 %collective-permute-start.7 = (bf16[384,512]{1,0:T(8,128)(2,1)}, bf16[384,512]{1,0:T(8,128)(2,1)}, u32[]{:S(2)}, u32[]{:S(2)}) collective-permute-start(bf16[384,512]{1,0:T(8,128)(2,1)} %collective-permute-done.6.r_4_.r_10_), channel_id=1, source_target_pairs={{0,14},{2,0},{4,2},{6,4},{8,6},{10,8},{12,10},{14,12},{1,15},{3,1}... | collective-permute-start | bytes 1179656 | tf_op jit(solution)/shard_map/ppermute | solution.py:38
  115.4 11.0 %collective-permute-start.18 = (bf16[400,512]{1,0:T(8,128)(2,1)S(1)}, bf16[400,512]{1,0:T(8,128)(2,1)S(1)}, u32[]{:S(2)}, u32[]{:S(2)}) collective-permute-start(bf16[400,512]{1,0:T(8,128)(2,1)S(1)} %get-tuple-element.63), channel_id=1, source_target_pairs={{0,2},{2,4},{4,6},{6,8},{8,10},{10,12},{12,14},{14,0},{1,3},{3,5},... | collective-permute-start | bytes 1228808 | tf_op jit(solution)/shard_map/ppermute | solution.py:33
  116.1 10.3 %collective-permute-start.19 = (bf16[400,512]{1,0:T(8,128)(2,1)S(1)}, bf16[400,512]{1,0:T(8,128)(2,1)S(1)}, u32[]{:S(2)}, u32[]{:S(2)}) collective-permute-start(bf16[400,512]{1,0:T(8,128)(2,1)S(1)} %get-tuple-element.64), channel_id=1, source_target_pairs={{0,14},{2,0},{4,2},{6,4},{8,6},{10,8},{12,10},{14,12},{1,15},{3,1}... | collective-permute-start | bytes 1228808 | tf_op jit(solution)/shard_map/ppermute | solution.py:38
  126.7 10.2 %collective-permute-start.20 = (bf16[400,512]{1,0:T(8,128)(2,1)S(1)}, bf16[400,512]{1,0:T(8,128)(2,1)S(1)}, u32[]{:S(2)}, u32[]{:S(2)}) collective-permute-start(bf16[400,512]{1,0:T(8,128)(2,1)S(1)} %get-tuple-element.65), channel_id=1, source_target_pairs={{0,2},{2,4},{4,6},{6,8},{8,10},{10,12},{12,14},{14,0},{1,3},{3,5},... | collective-permute-start | bytes 1228808 | tf_op jit(solution)/shard_map/ppermute | solution.py:33
  126.8 10.1 %collective-permute-start.21 = (bf16[400,512]{1,0:T(8,128)(2,1)S(1)}, bf16[400,512]{1,0:T(8,128)(2,1)S(1)}, u32[]{:S(2)}, u32[]{:S(2)}) collective-permute-start(bf16[400,512]{1,0:T(8,128)(2,1)S(1)} %get-tuple-element.66), channel_id=1, source_target_pairs={{0,14},{2,0},{4,2},{6,4},{8,6},{10,8},{12,10},{14,12},{1,15},{3,1}... | collective-permute-start | bytes 1228808 | tf_op jit(solution)/shard_map/ppermute | solution.py:38
  147.7 20.0 %all-to-all-start.2 = ((bf16[32,24,384]{2,1,0:T(8,128)(2,1)}), bf16[32,24,384]{2,1,0:T(8,128)(2,1)S(1)}, u32[]{:S(2)}, u32[]{:S(2)}) async-start(bf16[32,24,384]{2,1,0:T(8,128)(2,1)} %bitcast.9), calls=%async_computation.2 | async-start | bytes 1179648 | tf_op jit(solution)/shard_map/all_to_all | solution.py:707
  155.5 61.5 %collective-permute-start.32 = (bf16[3,4096,128]{2,1,0:T(8,128)(2,1)}, bf16[3,4096,128]{2,1,0:T(8,128)(2,1)}, u32[]{:S(2)}, u32[]{:S(2)}) collective-permute-start(bf16[3,4096,128]{2,1,0:T(8,128)(2,1)} %copy-done.10), channel_id=1, source_target_pairs={{0,1},{1,0},{2,3},{3,2},{4,5},{5,4},{6,7},{7,6},{8,9},{9,8},{10,11... | collective-permute-start | bytes 9437192 | tf_op jit(solution)/shard_map/ppermute | solution.py:47
  168.6 11.2 %collective-permute-start.27 = (bf16[256,256]{1,0:T(8,128)(2,1)S(1)}, bf16[256,256]{1,0:T(8,128)(2,1)S(1)}, u32[]{:S(2)}, u32[]{:S(2)}) collective-permute-start(bf16[256,256]{1,0:T(8,128)(2,1)S(1)} %fusion.4.refs_0_), channel_id=1, source_target_pairs={{0,4},{2,6},{4,8},{6,10},{8,12},{10,14},{12,0},{14,2},{1,5},{3,7},... | collective-permute-start | bytes 393224 | tf_op jit(solution)/shard_map/ppermute | solution.py:43
  171.7 11.6 %collective-permute-start.25 = (bf16[256,256]{1,0:T(8,128)(2,1)S(1)}, bf16[256,256]{1,0:T(8,128)(2,1)S(1)}, u32[]{:S(2)}, u32[]{:S(2)}) collective-permute-start(bf16[256,256]{1,0:T(8,128)(2,1)S(1)} %fusion.4.refs_0_), channel_id=1, source_target_pairs={{0,12},{2,14},{4,0},{6,2},{8,4},{10,6},{12,8},{14,10},{1,13},{3,15... | collective-permute-start | bytes 393224 | tf_op jit(solution)/shard_map/ppermute | solution.py:43
  174.4 10.5 %collective-permute-start.30 = (bf16[256,256]{1,0:T(8,128)(2,1)S(1)}, bf16[256,256]{1,0:T(8,128)(2,1)S(1)}, u32[]{:S(2)}, u32[]{:S(2)}) collective-permute-start(bf16[256,256]{1,0:T(8,128)(2,1)S(1)} %collective-permute-done.29.refs_7_), channel_id=1, source_target_pairs={{0,4},{2,6},{4,8},{6,10},{8,12},{10,14},{12,0},{14,2},{1,5},{3,7},... | collective-permute-start | bytes 393224 | tf_op jit(solution)/shard_map/ppermute | solution.py:43
  179.7 10.5 %collective-permute-start.28 = (bf16[256,256]{1,0:T(8,128)(2,1)S(1)}, bf16[256,256]{1,0:T(8,128)(2,1)S(1)}, u32[]{:S(2)}, u32[]{:S(2)}) collective-permute-start(bf16[256,256]{1,0:T(8,128)(2,1)S(1)} %collective-permute-done.27.refs_6_), channel_id=1, source_target_pairs={{0,4},{2,6},{4,8},{6,10},{8,12},{10,14},{12,0},{14,2},{1,5},{3,7},... | collective-permute-start | bytes 393224 | tf_op jit(solution)/shard_map/ppermute | solution.py:43
  179.7 10.5 %collective-permute-start.26 = (bf16[256,256]{1,0:T(8,128)(2,1)S(1)}, bf16[256,256]{1,0:T(8,128)(2,1)S(1)}, u32[]{:S(2)}, u32[]{:S(2)}) collective-permute-start(bf16[256,256]{1,0:T(8,128)(2,1)S(1)} %collective-permute-done.24.refs_1_), channel_id=1, source_target_pairs={{0,12},{2,14},{4,0},{6,2},{8,4},{10,6},{12,8},{14,10},{1,13},{3,15... | collective-permute-start | bytes 393224 | tf_op jit(solution)/shard_map/ppermute | solution.py:43
  199.5 11.5 %all-to-all-start.3 = ((f32[16,1,512]{2,1,0:T(1,128)}), f32[16,1,512]{2,1,0:T(1,128)S(1)}, u32[]{:S(2)}, u32[]{:S(2)}) async-start(f32[16,1,512]{2,1,0:T(1,128)} %broadcast_in_dim.17), calls=%async_computation.3 | async-start | bytes 65536 | tf_op jit(solution)/shard_map/all_to_all | solution.py:16
  211.1 21.2 %all-to-all-start.4 = ((bf16[16,128,256]{2,1,0:T(8,128)(2,1)}), bf16[16,128,256]{2,1,0:T(8,128)(2,1)}, u32[]{:S(2)}, u32[]{:S(2)}) async-start(bf16[16,128,256]{2,1,0:T(8,128)(2,1)} %outer.1), calls=%async_computation.4 | async-start | bytes 2097152 | tf_op jit(solution)/shard_map/all_to_all | solution.py:760
  215.7 13.2 %collective-permute-start.33 = (f32[32,128]{1,0:T(8,128)S(1)}, f32[32,128]{1,0:T(8,128)S(1)}, u32[]{:S(2)}, u32[]{:S(2)}) collective-permute-start(f32[32,128]{1,0:T(8,128)S(1)} %slice.46), channel_id=1, source_target_pairs={{16,0},{32,16},{48,32},{64,48},{80,64},{96,80},{112,96},{128,112},... | collective-permute-start | bytes 49160 | tf_op jit(solution)/shard_map/ppermute | solution.py:759
  (35 other events, 509.1 us)
where the time goes:
time: 236 us; the launch traced here: 234 us
  waiting for transfers between devices  82.1 us (35%)
  starting transfers between devices  81.9 us (35%)
  Pallas kernels  49.8 us (21%)
  local copies, waits for them, and re-layouts  10.5 us (4%)
  other arithmetic  8.41 us (4%)
    ppermute x11, waiting for transfers between devices, right(): return lax.ppermute(x, 'z', [(i, (i + 1) % n) for i in range(n)])  30 us
    ppermute x11, starting transfers between devices, left(): return lax.ppermute(x, 'z', [(i, (i - 1) % n) for i in range(n)])  28 us
    pallas_call x2, Pallas kernels, grads(): pl.pallas_call(lambda *r: grads_body(*r, n=n, add=add, offsets=offsets),...  15.2 us
    ppermute x7, waiting for transfers between devices, hops(): return lax.ppermute(x, 'z', [(i, (i + n_hops) % n) for i in range(n)])  12.9 us
    all_to_all x1, waiting for transfers between devices, per_device(): lax.all_to_all(sent.reshape(2 * experts, capacity, width_part), ('sp', 'c...  12.4 us
    all_to_all x1, waiting for transfers between devices, per_device(): lax.all_to_all(sent_back.reshape(2 * n_sp, half_cap, width_part + 128), (...  11 us
    pallas_call x2, Pallas kernels, project(): pl.pallas_call(lambda *r: project_body(*r, offsets=offsets, n=n, more=sta...  10.4 us
    ppermute x7, starting transfers between devices, hops(): return lax.ppermute(x, 'z', [(i, (i + n_hops) % n) for i in range(n)])  8.77 us
  transfers between devices with their start and end apart: 39, of which 20 were waited for; matrix products, arithmetic and copies ran while one was open for 5% of the time, Pallas kernels for 19%

commit v1 on v0

--- a/solution.py
+++ b/solution.py
@@ -393,7 +393,8 @@
     if add:
         old_h, gate, up, down, old, xbuf, cbuf, sems = refs
     else:
-        out, xbuf, cbuf, sems = refs
+        out, ready, xbuf, cbuf, sems = refs
+        ready[...] = jnp.zeros(ready.shape, F4)
     rows, width = x4.shape
     hid = act.shape[1]
     groups = []
@@ -442,7 +443,11 @@
         )
         out_specs = (VMEM,) * 3
     else:
-        out_shape, out_specs = jax.ShapeDtypeStruct((3, total, hid), BF), VMEM
+        out_shape = (
+            jax.ShapeDtypeStruct((3, total, hid), BF),
+            jax.ShapeDtypeStruct((8, 128), F4),
+        )
+        out_specs = (VMEM, VMEM)
     return pl.pallas_call(
         lambda *r: grads_body(*r, n=n, add=add, offsets=offsets),
         out_shape=out_shape,
@@ -691,8 +696,8 @@
         )(zs, parts, along, ra, la)
         ra, la = right(ra), left(la)
         if k == 2:
-            others = grads(zs, xs, x4, cb, b_oth, a_oth, None, offsets)
-            ra, la, others = lax.optimization_barrier((ra, la, others))
+            others, ready = grads(zs, xs, x4, cb, b_oth, a_oth, None, offsets)
+            ra, la, ready = lax.optimization_barrier((ra, la, ready))
     sent_back = pl.pallas_call(
         lambda *r: pack_body(*r, n_sp=n_sp),
         out_shape=jax.ShapeDtypeStruct((slot_count, width_part + 128), BF),

time: 236 us -> 237 us (level)
  transfers between devices with their start and end apart: 39 -> 39, of which waited for: 20 -> 18; matrix products, arithmetic and copies ran while one was open for 5% -> 5% of each run, Pallas kernels for 19% -> 19%
where the time goes in v1:
time: 237 us; the launch traced here: 234 us
  waiting for transfers between devices  81.6 us (34%)
  starting transfers between devices  80.8 us (34%)
  Pallas kernels  50.2 us (21%)
  local copies, waits for them, and re-layouts  11.8 us (5%)
  other arithmetic  8.41 us (4%)
    ppermute x11, waiting for transfers between devices, right(): return lax.ppermute(x, 'z', [(i, (i + 1) % n) for i in range(n)])  29.6 us
    ppermute x11, starting transfers between devices, left(): return lax.ppermute(x, 'z', [(i, (i - 1) % n) for i in range(n)])  28 us
    pallas_call x2, Pallas kernels, grads(): pl.pallas_call(lambda *r: grads_body(*r, n=n, add=add, offsets=offsets),...  15.6 us
    ppermute x7, waiting for transfers between devices, hops(): return lax.ppermute(x, 'z', [(i, (i + n_hops) % n) for i in range(n)])  13.2 us
    all_to_all x1, waiting for transfers between devices, per_device(): lax.all_to_all(sent.reshape(2 * experts, capacity, width_part), ('sp', 'c...  12.4 us
    all_to_all x1, waiting for transfers between devices, per_device(): lax.all_to_all(sent_back.reshape(2 * n_sp, half_cap, width_part + 128), (...  11 us
    pallas_call x2, Pallas kernels, project(): pl.pallas_call(lambda *r: project_body(*r, offsets=offsets, n=n, more=sta...  10.4 us
    unnamed x60, local copies, waits for them, and re-layouts  8.89 us
  transfers between devices with their start and end apart: 39, of which 18 were waited for; matrix products, arithmetic and copies ran while one was open for 5% of the time, Pallas kernels for 19%

profile of v1, /device:TPU:1, one launch (start us, length us, event | category | flops | bytes accessed | tf_op | source)
XLA Modules:
  0.0 234.3 jit_solution(14849554097150437256)
XLA Ops:
  0.6 3.3 %collective-permute-start.9 = (bf16[128,4096]{1,0:T(8,128)(2,1)}, bf16[128,4096]{1,0:T(8,128)(2,1)}, u32[]{:S(2)}, u32[]{:S(2)}) collective-permute-start(bf16[128,4096]{1,0:T(8,128)(2,1)} %bitcast.25), channel_id=1, source_target_pairs={{0,1},{1,0},{2,3},{3,2},{4,5},{5,4},{6,7},{7,6},{8,9},{9,8},{10,11... | collective-permute-start | bytes 3145736 | tf_op jit(solution)/shard_map/ppermute | solution.py:47
  7.1 3.4 %scatter.1 = (bf16[768,256]{1,0:T(8,128)(2,1)S(1)}, bf16[1536,256]{1,0:T(8,128)(2,1)}) custom-call(s32[2,256]{1,0:T(2,128)S(1)} %bitcast.29, f32[2,256]{1,0:T(2,128)S(1)} %bitcast.30, bf16[256,256]{1,0:T(8,128)(2,1)S(1)} %copy-done.4, bf16[256,256]{1,0:T(8,128)(2,1)S(1)} %copy-done.1), custom_call_target="tpu_custom_call" | custom-call | tf_op jit(solution)/shard_map/scatter/pallas_call | solution.py:561
  11.3 5.5 %all-to-all-start = ((bf16[32,48,256]{2,1,0:T(8,128)(2,1)}), bf16[32,48,256]{2,1,0:T(8,128)(2,1)}, u32[]{:S(2)}, u32[]{:S(2)}) async-start(bf16[32,48,256]{2,1,0:T(8,128)(2,1)} %bitcast.2), calls=%async_computation | async-start | bytes 1572864 | tf_op jit(solution)/shard_map/all_to_all | solution.py:579
  18.7 12.4 %all-to-all-done = bf16[32,48,256]{2,1,0:T(8,128)(2,1)} async-done(((bf16[32,48,256]{2,1,0:T(8,128)(2,1)}), bf16[32,48,256]{2,1,0:T(8,128)(2,1)}, u32[]{:S(2)}, u32[]{:S(2)}) %all-to-all-start) | async-done | bytes 786464 | tf_op jit(solution)/shard_map/all_to_all | solution.py:579
  34.7 3.9 %collective-permute-start.4 = (bf16[384,512]{1,0:T(8,128)(2,1)}, bf16[384,512]{1,0:T(8,128)(2,1)}, u32[]{:S(2)}, u32[]{:S(2)}) collective-permute-start(bf16[384,512]{1,0:T(8,128)(2,1)} %get-tuple-element.51.r_6_.r_4_), channel_id=1, source_target_pairs={{0,14},{2,0},{4,2},{6,4},{8,6},{10,8},{12,10},{14,12},{1,15},{3,1}... | collective-permute-start | bytes 1179656 | tf_op jit(solution)/shard_map/ppermute | solution.py:38
  42.2 5.5 %collective-permute-done.r_2_ = bf16[384,512]{1,0:T(8,128)(2,1)} collective-permute-done((bf16[384,512]{1,0:T(8,128)(2,1)S(1)}, bf16[384,512]{1,0:T(8,128)(2,1)}, u32[]{:S(2)}, u32[]{:S(2)}) %collective-permute-start) | collective-permute-done | bytes 393248 | tf_op jit(solution)/shard_map/ppermute | solution.py:33
  47.7 2.7 %collective-permute-start.5 = (bf16[384,512]{1,0:T(8,128)(2,1)}, bf16[384,512]{1,0:T(8,128)(2,1)}, u32[]{:S(2)}, u32[]{:S(2)}) collective-permute-start(bf16[384,512]{1,0:T(8,128)(2,1)} %collective-permute-done.4.r_8_.r_6_), channel_id=1, source_target_pairs={{0,14},{2,0},{4,2},{6,4},{8,6},{10,8},{12,10},{14,12},{1,15},{3,1}... | collective-permute-start | bytes 1179656 | tf_op jit(solution)/shard_map/ppermute | solution.py:38
  50.5 4.7 %collective-permute-done.10.r_3_ = bf16[384,512]{1,0:T(8,128)(2,1)} collective-permute-done((bf16[384,512]{1,0:T(8,128)(2,1)S(1)}, bf16[384,512]{1,0:T(8,128)(2,1)}, u32[]{:S(2)}, u32[]{:S(2)}) %collective-permute-start.10) | collective-permute-done | bytes 393248 | tf_op jit(solution)/shard_map/ppermute | solution.py:38
  55.2 3.5 %collective-permute-start.11 = (bf16[384,512]{1,0:T(8,128)(2,1)}, bf16[384,512]{1,0:T(8,128)(2,1)}, u32[]{:S(2)}, u32[]{:S(2)}) collective-permute-start(bf16[384,512]{1,0:T(8,128)(2,1)} %collective-permute-done.10.r_3_), channel_id=1, source_target_pairs={{0,14},{2,0},{4,2},{6,4},{8,6},{10,8},{12,10},{14,12},{1,15},{3,1}... | collective-permute-start | bytes 1179656 | tf_op jit(solution)/shard_map/ppermute | solution.py:38
  58.7 5.8 %collective-permute-done.1.r_4_ = bf16[384,512]{1,0:T(8,128)(2,1)} collective-permute-done((bf16[384,512]{1,0:T(8,128)(2,1)}, bf16[384,512]{1,0:T(8,128)(2,1)}, u32[]{:S(2)}, u32[]{:S(2)}) %collective-permute-start.1) | collective-permute-done | bytes 393248 | tf_op jit(solution)/shard_map/ppermute | solution.py:33
  64.5 2.7 %collective-permute-start.6 = (bf16[384,512]{1,0:T(8,128)(2,1)}, bf16[384,512]{1,0:T(8,128)(2,1)}, u32[]{:S(2)}, u32[]{:S(2)}) collective-permute-start(bf16[384,512]{1,0:T(8,128)(2,1)} %collective-permute-done.5.r_10_.r_8_), channel_id=1, source_target_pairs={{0,14},{2,0},{4,2},{6,4},{8,6},{10,8},{12,10},{14,12},{1,15},{3,1}... | collective-permute-start | bytes 1179656 | tf_op jit(solution)/shard_map/ppermute | solution.py:38
  67.9 8.4 %all-to-all-start.1 = ((f32[16,1,1792]{2,1,0:T(1,128)}), f32[16,1,1792]{2,1,0:T(1,128)}, u32[]{:S(2)}, u32[]{:S(2)}) async-start(f32[16,1,1792]{2,1,0:T(1,128)} %broadcast_in_dim.15), calls=%async_computation.1 | async-start | bytes 229376 | tf_op jit(solution)/shard_map/all_to_all | solution.py:609
  81.5 3.6 %collective-permute-start.7 = (bf16[384,512]{1,0:T(8,128)(2,1)}, bf16[384,512]{1,0:T(8,128)(2,1)}, u32[]{:S(2)}, u32[]{:S(2)}) collective-permute-start(bf16[384,512]{1,0:T(8,128)(2,1)} %collective-permute-done.6.r_4_.r_10_), channel_id=1, source_target_pairs={{0,14},{2,0},{4,2},{6,4},{8,6},{10,8},{12,10},{14,12},{1,15},{3,1}... | collective-permute-start | bytes 1179656 | tf_op jit(solution)/shard_map/ppermute | solution.py:38
  90.7 6.7 %project.2 = (f32[384,256]{1,0:T(8,128)S(1)}, f32[384,256]{1,0:T(8,128)S(1)}, f32[384,256]{1,0:T(8,128)S(1)}, bf16[1920,512]{1,0:T(8,128)(2,1)S(1)}) custom-call(s32[1]{0:T(128)} %bitcast.4.r_0_, bf16[384,512]{1,0:T(8,128)(2,1)S(1)} %get-tuple-element.49.r_1_, bf16[384,512]{1,0:T(8,128)(2,1)} %collective-permute-done.r_2_, ...), custom_call_target="tpu_custom_call" | custom-call | tf_op jit(solution)/shard_map/project/pallas_call | solution.py:210
  97.5 3.7 %project.3 = (f32[384,256]{1,0:T(8,128)S(1)}, f32[384,256]{1,0:T(8,128)S(1)}, f32[384,256]{1,0:T(8,128)S(1)}, bf16[768,512]{1,0:T(8,128)(2,1)S(1)}) custom-call(s32[1]{0:T(128)} %bitcast.4.r_0_, bf16[384,512]{1,0:T(8,128)(2,1)} %collective-permute-done.2.r_1_, bf16[384,512]{1,0:T(8,128)(2,1)} %collective-permute-done.12.r_2_, ...), custom_call_target="tpu_custom_call" | custom-call | tf_op jit(solution)/shard_map/project/pallas_call | solution.py:210
  101.2 4.5 %finish.1 = (bf16[384,512]{1,0:T(8,128)(2,1)S(1)}, bf16[384,256]{1,0:T(8,128)(2,1)S(1)}, bf16[384,256]{1,0:T(8,128)(2,1)S(1)}, bf16[384,128]{1,0:T(8,128)(2,1)S(...) custom-call(s32[1]{0:T(128)} %bitcast.4.r_0_, ...), custom_call_target="tpu_custom_call" | custom-call | tf_op jit(solution)/shard_map/finish/pallas_call | solution.py:643
  105.8 3.4 %collective-permute-start.16 = (bf16[208,512]{1,0:T(8,128)(2,1)S(1)}, bf16[208,512]{1,0:T(8,128)(2,1)S(1)}, u32[]{:S(2)}, u32[]{:S(2)}) collective-permute-start(bf16[208,512]{1,0:T(8,128)(2,1)S(1)} %get-tuple-element.61), channel_id=1, source_target_pairs={{0,2},{2,4},{4,6},{6,8},{8,10},{10,12},{12,14},{14,0},{1,3},{3,5},... | collective-permute-start | bytes 638984 | tf_op jit(solution)/shard_map/ppermute | solution.py:33
  109.2 4.3 %parts.1.r_1_ = bf16[384,4096]{1,0:T(8,128)(2,1)S(1)} custom-call(bf16[384,256]{1,0:T(8,128)(2,1)S(1)} %get-tuple-element.58.r_0_.r_12_, bf16[384,256]{1,0:T(8,128)(2,1)S(1)} %get-tuple-element.59.r_1_.r_12_, bf16[4096,256]{1,0:T(8,128)(2,1)S(1)} %pad_maximum_fusion.r_11_.r_5_.r_3_.r_2_, bf16[4096,256]{1,0:T(8,128)(2,1)} %collective-permute-done.8.r_12_.r_6_.r_4_.r_3_), custom_call_target="tpu_custom_call" | custom-call | tf_op jit(solution)/shard_map/parts/pallas_call | solution.py:674
  118.1 8.3 %collective-permute-done.18.r_3_ = bf16[400,512]{1,0:T(8,128)(2,1)S(1)} collective-permute-done((bf16[400,512]{1,0:T(8,128)(2,1)S(1)}, bf16[400,512]{1,0:T(8,128)(2,1)S(1)}, u32[]{:S(2)}, u32[]{:S(2)}) %collective-permute-start.18) | collective-permute-done | bytes 409632 | tf_op jit(solution)/shard_map/ppermute | solution.py:33
  129.4 7.4 %collective-permute-done.20.r_3_ = bf16[400,512]{1,0:T(8,128)(2,1)S(1)} collective-permute-done((bf16[400,512]{1,0:T(8,128)(2,1)S(1)}, bf16[400,512]{1,0:T(8,128)(2,1)S(1)}, u32[]{:S(2)}, u32[]{:S(2)}) %collective-permute-start.20) | collective-permute-done | bytes 409632 | tf_op jit(solution)/shard_map/ppermute | solution.py:33
  139.8 6.2 %grads_other.1 = (bf16[3,4096,128]{2,1,0:T(8,128)(2,1)S(1)}, f32[8,128]{1,0:T(8,128)}) custom-call(s32[1]{0:T(128)} %bitcast.4.r_0_, bf16[1920,512]{1,0:T(8,128)(2,1)S(1)} %get-tuple-element.71.r_1_, bf16[768,512]{1,0:T(8,128)(2,1)S(1)} %get-tuple-element.72.r_2_, bf16[384,512]{1,0:T(8,128)(2,1)S(1)} %get-tuple-element.73.r_3_, ...), custom_call_target="tpu_custom_call" | custom-call | flops 4831838208 | bytes 16777216 | tf_op jit(solution)/shard_map/grads_other/pallas_call | solution.py:451
  149.0 7.5 %all-to-all-start.2 = ((bf16[32,24,384]{2,1,0:T(8,128)(2,1)}), bf16[32,24,384]{2,1,0:T(8,128)(2,1)S(1)}, u32[]{:S(2)}, u32[]{:S(2)}) async-start(bf16[32,24,384]{2,1,0:T(8,128)(2,1)} %bitcast.9), calls=%async_computation.2 | async-start | bytes 1179648 | tf_op jit(solution)/shard_map/all_to_all | solution.py:712
  157.7 11.0 %all-to-all-done.2 = bf16[32,24,384]{2,1,0:T(8,128)(2,1)S(1)} async-done(((bf16[32,24,384]{2,1,0:T(8,128)(2,1)}), bf16[32,24,384]{2,1,0:T(8,128)(2,1)S(1)}, u32[]{:S(2)}, u32[]{:S(2)}) %all-to-all-start.2) | async-done | bytes 589856 | tf_op jit(solution)/shard_map/all_to_all | solution.py:712
  175.4 4.7 %collective-permute-done.27.refs_6_ = bf16[256,256]{1,0:T(8,128)(2,1)S(1)} collective-permute-done((bf16[256,256]{1,0:T(8,128)(2,1)S(1)}, bf16[256,256]{1,0:T(8,128)(2,1)S(1)}, u32[]{:S(2)}, u32[]{:S(2)}) %collective-permute-start.27) | collective-permute-done | bytes 131104 | tf_op jit(solution)/shard_map/ppermute | solution.py:43
  180.1 3.6 %collective-permute-start.26 = (bf16[256,256]{1,0:T(8,128)(2,1)S(1)}, bf16[256,256]{1,0:T(8,128)(2,1)S(1)}, u32[]{:S(2)}, u32[]{:S(2)}) collective-permute-start(bf16[256,256]{1,0:T(8,128)(2,1)S(1)} %collective-permute-done.24.refs_1_), channel_id=1, source_target_pairs={{0,12},{2,14},{4,0},{6,2},{8,4},{10,6},{12,8},{14,10},{1,13},{3,15... | collective-permute-start | bytes 393224 | tf_op jit(solution)/shard_map/ppermute | solution.py:43
  183.7 7.7 %collective-permute-done.28.refs_4_ = bf16[256,256]{1,0:T(8,128)(2,1)S(1)} collective-permute-done((bf16[256,256]{1,0:T(8,128)(2,1)S(1)}, bf16[256,256]{1,0:T(8,128)(2,1)S(1)}, u32[]{:S(2)}, u32[]{:S(2)}) %collective-permute-start.28) | collective-permute-done | bytes 131104 | tf_op jit(solution)/shard_map/ppermute | solution.py:43
  191.4 2.7 %collective-permute-start.31 = (bf16[8,256,256]{2,1,0:T(8,128)(2,1)S(1)}, bf16[8,256,256]{2,1,0:T(8,128)(2,1)S(1)}, u32[]{:S(2)}, u32[]{:S(2)}) collective-permute-start(bf16[8,256,256]{2,1,0:T(8,128)(2,1)S(1)} %bitcast.22), channel_id=1, source_target_pairs={{0,1},{1,0},{2,3},{3,2},{4,5},{5,4},{6,7},{7,6},{8,9},{9,8},{10,11... | collective-permute-start | bytes 3145736 | tf_op jit(solution)/shard_map/ppermute | solution.py:47
  199.8 3.7 %all-to-all-start.3 = ((f32[16,1,512]{2,1,0:T(1,128)}), f32[16,1,512]{2,1,0:T(1,128)S(1)}, u32[]{:S(2)}, u32[]{:S(2)}) async-start(f32[16,1,512]{2,1,0:T(1,128)} %broadcast_in_dim.17), calls=%async_computation.3 | async-start | bytes 65536 | tf_op jit(solution)/shard_map/all_to_all | solution.py:16
  203.6 3.1 %outer.1 = bf16[16,128,256]{2,1,0:T(8,128)(2,1)} custom-call(s32[2]{0:T(128)S(1)} %pad_add_fusion.r_0_, bf16[8,256,256]{2,1,0:T(8,128)(2,1)S(1)} %bitcast.24, bf16[8,256,256]{2,1,0:T(8,128)(2,1)S(1)} %collective-permute-done.31.r_2_, bf16[128,256]{1,0:T(8,128)(2,1)S(1)} %copy.37.r_3_), custom_call_target="tpu_custom_call" | custom-call | tf_op jit(solution)/shard_map/outer/pallas_call | solution.py:752
  206.8 4.2 %all-to-all-done.3 = f32[16,1,512]{2,1,0:T(1,128)S(1)} async-done(((f32[16,1,512]{2,1,0:T(1,128)}), f32[16,1,512]{2,1,0:T(1,128)S(1)}, u32[]{:S(2)}, u32[]{:S(2)}) %all-to-all-start.3) | async-done | bytes 32800 | tf_op jit(solution)/shard_map/all_to_all | solution.py:16
  211.0 4.9 %all-to-all-start.4 = ((bf16[16,128,256]{2,1,0:T(8,128)(2,1)}), bf16[16,128,256]{2,1,0:T(8,128)(2,1)}, u32[]{:S(2)}, u32[]{:S(2)}) async-start(bf16[16,128,256]{2,1,0:T(8,128)(2,1)} %outer.1), calls=%async_computation.4 | async-start | bytes 2097152 | tf_op jit(solution)/shard_map/all_to_all | solution.py:765
  218.5 9.4 %grads_own.1 = (f32[4096,128]{1,0:T(8,128)}, f32[4096,128]{1,0:T(8,128)}, f32[128,4096]{1,0:T(8,128)}) custom-call(s32[1]{0:T(128)} %bitcast.4.r_0_, bf16[1920,512]{1,0:T(8,128)(2,1)S(1)} %copy-done.12, bf16[768,512]{1,0:T(8,128)(2,1)S(1)} %copy-done.14, bf16[384,512]{1,0:T(8,128)(2,1)S(1)} %copy-done.16, bf16[384,512]{1,0:T(8,128)(2,1)} %get-tuple-element.51.r_6_.r_4_, ...), custom_call_target="tpu_custom_call" | custom-call | flops 4831838208 | bytes 16777216 | tf_op jit(solution)/shard_map/grads_own/pallas_call | solution.py:451
  (152 shorter events, 60.6 us)
Async XLA Ops:
  0.6 41.5 %collective-permute-start.9 = (bf16[128,4096]{1,0:T(8,128)(2,1)}, bf16[128,4096]{1,0:T(8,128)(2,1)}, u32[]{:S(2)}, u32[]{:S(2)}) collective-permute-start(bf16[128,4096]{1,0:T(8,128)(2,1)} %bitcast.25), channel_id=1, source_target_pairs={{0,1},{1,0},{2,3},{3,2},{4,5},{5,4},{6,7},{7,6},{8,9},{9,8},{10,11... | collective-permute-start | bytes 3145736 | tf_op jit(solution)/shard_map/ppermute | solution.py:47
  11.3 19.8 %all-to-all-start = ((bf16[32,48,256]{2,1,0:T(8,128)(2,1)}), bf16[32,48,256]{2,1,0:T(8,128)(2,1)}, u32[]{:S(2)}, u32[]{:S(2)}) async-start(bf16[32,48,256]{2,1,0:T(8,128)(2,1)} %bitcast.2), calls=%async_computation | async-start | bytes 1572864 | tf_op jit(solution)/shard_map/all_to_all | solution.py:579
  18.3 72.0 %collective-permute-start.8 = (bf16[4096,256]{1,0:T(8,128)(2,1)S(1)}, bf16[4096,256]{1,0:T(8,128)(2,1)}, u32[]{:S(2)}, u32[]{:S(2)}) collective-permute-start(bf16[4096,256]{1,0:T(8,128)(2,1)S(1)} %pad_maximum_fusion.r_11_.r_5_.r_3_.r_2_), channel_id=1, source_target_pairs={{0,1},{1,0},{2,3},{3,2},{4,5},{5,4},{6,7},{7,6},{8,9},{9,8},{10,11... | collective-permute-start | bytes 6291464 | tf_op jit(solution)/shard_map/ppermute | solution.py:47
  33.0 14.7 %collective-permute-start = (bf16[384,512]{1,0:T(8,128)(2,1)S(1)}, bf16[384,512]{1,0:T(8,128)(2,1)}, u32[]{:S(2)}, u32[]{:S(2)}) collective-permute-start(bf16[384,512]{1,0:T(8,128)(2,1)S(1)} %get-tuple-element.49.r_1_), channel_id=1, source_target_pairs={{0,2},{2,4},{4,6},{6,8},{8,10},{10,12},{12,14},{14,0},{1,3},{3,5},... | collective-permute-start | bytes 1179656 | tf_op jit(solution)/shard_map/ppermute | solution.py:33
  34.7 13.0 %collective-permute-start.4 = (bf16[384,512]{1,0:T(8,128)(2,1)}, bf16[384,512]{1,0:T(8,128)(2,1)}, u32[]{:S(2)}, u32[]{:S(2)}) collective-permute-start(bf16[384,512]{1,0:T(8,128)(2,1)} %get-tuple-element.51.r_6_.r_4_), channel_id=1, source_target_pairs={{0,14},{2,0},{4,2},{6,4},{8,6},{10,8},{12,10},{14,12},{1,15},{3,1}... | collective-permute-start | bytes 1179656 | tf_op jit(solution)/shard_map/ppermute | solution.py:38
  40.6 14.6 %collective-permute-start.10 = (bf16[384,512]{1,0:T(8,128)(2,1)S(1)}, bf16[384,512]{1,0:T(8,128)(2,1)}, u32[]{:S(2)}, u32[]{:S(2)}) collective-permute-start(bf16[384,512]{1,0:T(8,128)(2,1)S(1)} %get-tuple-element.49.r_1_), channel_id=1, source_target_pairs={{0,14},{2,0},{4,2},{6,4},{8,6},{10,8},{12,10},{14,12},{1,15},{3,1}... | collective-permute-start | bytes 1179656 | tf_op jit(solution)/shard_map/ppermute | solution.py:38
  42.2 16.5 %collective-permute-start.13 = (bf16[384,512]{1,0:T(8,128)(2,1)}, bf16[384,512]{1,0:T(8,128)(2,1)}, u32[]{:S(2)}, u32[]{:S(2)}) collective-permute-start(bf16[384,512]{1,0:T(8,128)(2,1)} %get-tuple-element.51.r_6_.r_4_), channel_id=1, source_target_pairs={{0,2},{2,4},{4,6},{6,8},{8,10},{10,12},{12,14},{14,0},{1,3},{3,5},... | collective-permute-start | bytes 1179656 | tf_op jit(solution)/shard_map/ppermute | solution.py:33
  47.7 16.9 %collective-permute-start.1 = (bf16[384,512]{1,0:T(8,128)(2,1)}, bf16[384,512]{1,0:T(8,128)(2,1)}, u32[]{:S(2)}, u32[]{:S(2)}) collective-permute-start(bf16[384,512]{1,0:T(8,128)(2,1)} %collective-permute-done.r_2_), channel_id=1, source_target_pairs={{0,2},{2,4},{4,6},{6,8},{8,10},{10,12},{12,14},{14,0},{1,3},{3,5},... | collective-permute-start | bytes 1179656 | tf_op jit(solution)/shard_map/ppermute | solution.py:33
  47.7 16.9 %collective-permute-start.5 = (bf16[384,512]{1,0:T(8,128)(2,1)}, bf16[384,512]{1,0:T(8,128)(2,1)}, u32[]{:S(2)}, u32[]{:S(2)}) collective-permute-start(bf16[384,512]{1,0:T(8,128)(2,1)} %collective-permute-done.4.r_8_.r_6_), channel_id=1, source_target_pairs={{0,14},{2,0},{4,2},{6,4},{8,6},{10,8},{12,10},{14,12},{1,15},{3,1}... | collective-permute-start | bytes 1179656 | tf_op jit(solution)/shard_map/ppermute | solution.py:38
  55.2 21.2 %collective-permute-start.11 = (bf16[384,512]{1,0:T(8,128)(2,1)}, bf16[384,512]{1,0:T(8,128)(2,1)}, u32[]{:S(2)}, u32[]{:S(2)}) collective-permute-start(bf16[384,512]{1,0:T(8,128)(2,1)} %collective-permute-done.10.r_3_), channel_id=1, source_target_pairs={{0,14},{2,0},{4,2},{6,4},{8,6},{10,8},{12,10},{14,12},{1,15},{3,1}... | collective-permute-start | bytes 1179656 | tf_op jit(solution)/shard_map/ppermute | solution.py:38
  58.7 20.3 %collective-permute-start.14 = (bf16[384,512]{1,0:T(8,128)(2,1)}, bf16[384,512]{1,0:T(8,128)(2,1)}, u32[]{:S(2)}, u32[]{:S(2)}) collective-permute-start(bf16[384,512]{1,0:T(8,128)(2,1)} %collective-permute-done.13.r_7_.r_5_), channel_id=1, source_target_pairs={{0,2},{2,4},{4,6},{6,8},{8,10},{10,12},{12,14},{14,0},{1,3},{3,5},... | collective-permute-start | bytes 1179656 | tf_op jit(solution)/shard_map/ppermute | solution.py:33
  64.5 16.7 %collective-permute-start.2 = (bf16[384,512]{1,0:T(8,128)(2,1)}, bf16[384,512]{1,0:T(8,128)(2,1)}, u32[]{:S(2)}, u32[]{:S(2)}) collective-permute-start(bf16[384,512]{1,0:T(8,128)(2,1)} %collective-permute-done.1.r_4_), channel_id=1, source_target_pairs={{0,2},{2,4},{4,6},{6,8},{8,10},{10,12},{12,14},{14,0},{1,3},{3,5},... | collective-permute-start | bytes 1179656 | tf_op jit(solution)/shard_map/ppermute | solution.py:33
  64.5 17.0 %collective-permute-start.6 = (bf16[384,512]{1,0:T(8,128)(2,1)}, bf16[384,512]{1,0:T(8,128)(2,1)}, u32[]{:S(2)}, u32[]{:S(2)}) collective-permute-start(bf16[384,512]{1,0:T(8,128)(2,1)} %collective-permute-done.5.r_10_.r_8_), channel_id=1, source_target_pairs={{0,14},{2,0},{4,2},{6,4},{8,6},{10,8},{12,10},{14,12},{1,15},{3,1}... | collective-permute-start | bytes 1179656 | tf_op jit(solution)/shard_map/ppermute | solution.py:38
  67.9 18.4 %all-to-all-start.1 = ((f32[16,1,1792]{2,1,0:T(1,128)}), f32[16,1,1792]{2,1,0:T(1,128)}, u32[]{:S(2)}, u32[]{:S(2)}) async-start(f32[16,1,1792]{2,1,0:T(1,128)} %broadcast_in_dim.15), calls=%async_computation.1 | async-start | bytes 229376 | tf_op jit(solution)/shard_map/all_to_all | solution.py:609
  76.4 21.1 %collective-permute-start.12 = (bf16[384,512]{1,0:T(8,128)(2,1)}, bf16[384,512]{1,0:T(8,128)(2,1)}, u32[]{:S(2)}, u32[]{:S(2)}) collective-permute-start(bf16[384,512]{1,0:T(8,128)(2,1)} %collective-permute-done.11.r_5_), channel_id=1, source_target_pairs={{0,14},{2,0},{4,2},{6,4},{8,6},{10,8},{12,10},{14,12},{1,15},{3,1}... | collective-permute-start | bytes 1179656 | tf_op jit(solution)/shard_map/ppermute | solution.py:38
  79.0 18.4 %collective-permute-start.15 = (bf16[384,512]{1,0:T(8,128)(2,1)}, bf16[384,512]{1,0:T(8,128)(2,1)}, u32[]{:S(2)}, u32[]{:S(2)}) collective-permute-start(bf16[384,512]{1,0:T(8,128)(2,1)} %collective-permute-done.14.r_9_.r_7_), channel_id=1, source_target_pairs={{0,2},{2,4},{4,6},{6,8},{8,10},{10,12},{12,14},{14,0},{1,3},{3,5},... | collective-permute-start | bytes 1179656 | tf_op jit(solution)/shard_map/ppermute | solution.py:33
  81.3 19.9 %collective-permute-start.3 = (bf16[384,512]{1,0:T(8,128)(2,1)}, bf16[384,512]{1,0:T(8,128)(2,1)}, u32[]{:S(2)}, u32[]{:S(2)}) collective-permute-start(bf16[384,512]{1,0:T(8,128)(2,1)} %collective-permute-done.2.r_1_), channel_id=1, source_target_pairs={{0,2},{2,4},{4,6},{6,8},{8,10},{10,12},{12,14},{14,0},{1,3},{3,5},... | collective-permute-start | bytes 1179656 | tf_op jit(solution)/shard_map/ppermute | solution.py:33
  81.5 19.7 %collective-permute-start.7 = (bf16[384,512]{1,0:T(8,128)(2,1)}, bf16[384,512]{1,0:T(8,128)(2,1)}, u32[]{:S(2)}, u32[]{:S(2)}) collective-permute-start(bf16[384,512]{1,0:T(8,128)(2,1)} %collective-permute-done.6.r_4_.r_10_), channel_id=1, source_target_pairs={{0,14},{2,0},{4,2},{6,4},{8,6},{10,8},{12,10},{14,12},{1,15},{3,1}... | collective-permute-start | bytes 1179656 | tf_op jit(solution)/shard_map/ppermute | solution.py:38
  115.4 11.0 %collective-permute-start.18 = (bf16[400,512]{1,0:T(8,128)(2,1)S(1)}, bf16[400,512]{1,0:T(8,128)(2,1)S(1)}, u32[]{:S(2)}, u32[]{:S(2)}) collective-permute-start(bf16[400,512]{1,0:T(8,128)(2,1)S(1)} %get-tuple-element.63), channel_id=1, source_target_pairs={{0,2},{2,4},{4,6},{6,8},{8,10},{10,12},{12,14},{14,0},{1,3},{3,5},... | collective-permute-start | bytes 1228808 | tf_op jit(solution)/shard_map/ppermute | solution.py:33
  116.1 10.3 %collective-permute-start.19 = (bf16[400,512]{1,0:T(8,128)(2,1)S(1)}, bf16[400,512]{1,0:T(8,128)(2,1)S(1)}, u32[]{:S(2)}, u32[]{:S(2)}) collective-permute-start(bf16[400,512]{1,0:T(8,128)(2,1)S(1)} %get-tuple-element.64), channel_id=1, source_target_pairs={{0,14},{2,0},{4,2},{6,4},{8,6},{10,8},{12,10},{14,12},{1,15},{3,1}... | collective-permute-start | bytes 1228808 | tf_op jit(solution)/shard_map/ppermute | solution.py:38
  126.7 10.2 %collective-permute-start.20 = (bf16[400,512]{1,0:T(8,128)(2,1)S(1)}, bf16[400,512]{1,0:T(8,128)(2,1)S(1)}, u32[]{:S(2)}, u32[]{:S(2)}) collective-permute-start(bf16[400,512]{1,0:T(8,128)(2,1)S(1)} %get-tuple-element.65), channel_id=1, source_target_pairs={{0,2},{2,4},{4,6},{6,8},{8,10},{10,12},{12,14},{14,0},{1,3},{3,5},... | collective-permute-start | bytes 1228808 | tf_op jit(solution)/shard_map/ppermute | solution.py:33
  126.7 10.1 %collective-permute-start.21 = (bf16[400,512]{1,0:T(8,128)(2,1)S(1)}, bf16[400,512]{1,0:T(8,128)(2,1)S(1)}, u32[]{:S(2)}, u32[]{:S(2)}) collective-permute-start(bf16[400,512]{1,0:T(8,128)(2,1)S(1)} %get-tuple-element.66), channel_id=1, source_target_pairs={{0,14},{2,0},{4,2},{6,4},{8,6},{10,8},{12,10},{14,12},{1,15},{3,1}... | collective-permute-start | bytes 1228808 | tf_op jit(solution)/shard_map/ppermute | solution.py:38
  137.2 10.5 %collective-permute-start.23 = (bf16[400,512]{1,0:T(8,128)(2,1)S(1)}, bf16[400,512]{1,0:T(8,128)(2,1)S(1)}, u32[]{:S(2)}, u32[]{:S(2)}) collective-permute-start(bf16[400,512]{1,0:T(8,128)(2,1)S(1)} %get-tuple-element.70), channel_id=1, source_target_pairs={{0,14},{2,0},{4,2},{6,4},{8,6},{10,8},{12,10},{14,12},{1,15},{3,1}... | collective-permute-start | bytes 1228808 | tf_op jit(solution)/shard_map/ppermute | solution.py:38
  149.0 19.7 %all-to-all-start.2 = ((bf16[32,24,384]{2,1,0:T(8,128)(2,1)}), bf16[32,24,384]{2,1,0:T(8,128)(2,1)S(1)}, u32[]{:S(2)}, u32[]{:S(2)}) async-start(bf16[32,24,384]{2,1,0:T(8,128)(2,1)} %bitcast.9), calls=%async_computation.2 | async-start | bytes 1179648 | tf_op jit(solution)/shard_map/all_to_all | solution.py:712
  156.5 61.0 %collective-permute-start.32 = (bf16[3,4096,128]{2,1,0:T(8,128)(2,1)}, bf16[3,4096,128]{2,1,0:T(8,128)(2,1)}, u32[]{:S(2)}, u32[]{:S(2)}) collective-permute-start(bf16[3,4096,128]{2,1,0:T(8,128)(2,1)} %copy-done.10), channel_id=1, source_target_pairs={{0,1},{1,0},{2,3},{3,2},{4,5},{5,4},{6,7},{7,6},{8,9},{9,8},{10,11... | collective-permute-start | bytes 9437192 | tf_op jit(solution)/shard_map/ppermute | solution.py:47
  169.5 10.6 %collective-permute-start.27 = (bf16[256,256]{1,0:T(8,128)(2,1)S(1)}, bf16[256,256]{1,0:T(8,128)(2,1)S(1)}, u32[]{:S(2)}, u32[]{:S(2)}) collective-permute-start(bf16[256,256]{1,0:T(8,128)(2,1)S(1)} %fusion.4.refs_0_), channel_id=1, source_target_pairs={{0,4},{2,6},{4,8},{6,10},{8,12},{10,14},{12,0},{14,2},{1,5},{3,7},... | collective-permute-start | bytes 393224 | tf_op jit(solution)/shard_map/ppermute | solution.py:43
  172.2 11.5 %collective-permute-start.25 = (bf16[256,256]{1,0:T(8,128)(2,1)S(1)}, bf16[256,256]{1,0:T(8,128)(2,1)S(1)}, u32[]{:S(2)}, u32[]{:S(2)}) collective-permute-start(bf16[256,256]{1,0:T(8,128)(2,1)S(1)} %fusion.4.refs_0_), channel_id=1, source_target_pairs={{0,12},{2,14},{4,0},{6,2},{8,4},{10,6},{12,8},{14,10},{1,13},{3,15... | collective-permute-start | bytes 393224 | tf_op jit(solution)/shard_map/ppermute | solution.py:43
  180.1 11.2 %collective-permute-start.28 = (bf16[256,256]{1,0:T(8,128)(2,1)S(1)}, bf16[256,256]{1,0:T(8,128)(2,1)S(1)}, u32[]{:S(2)}, u32[]{:S(2)}) collective-permute-start(bf16[256,256]{1,0:T(8,128)(2,1)S(1)} %collective-permute-done.27.refs_6_), channel_id=1, source_target_pairs={{0,4},{2,6},{4,8},{6,10},{8,12},{10,14},{12,0},{14,2},{1,5},{3,7},... | collective-permute-start | bytes 393224 | tf_op jit(solution)/shard_map/ppermute | solution.py:43
  180.1 11.2 %collective-permute-start.26 = (bf16[256,256]{1,0:T(8,128)(2,1)S(1)}, bf16[256,256]{1,0:T(8,128)(2,1)S(1)}, u32[]{:S(2)}, u32[]{:S(2)}) collective-permute-start(bf16[256,256]{1,0:T(8,128)(2,1)S(1)} %collective-permute-done.24.refs_1_), channel_id=1, source_target_pairs={{0,12},{2,14},{4,0},{6,2},{8,4},{10,6},{12,8},{14,10},{1,13},{3,15... | collective-permute-start | bytes 393224 | tf_op jit(solution)/shard_map/ppermute | solution.py:43
  199.8 11.1 %all-to-all-start.3 = ((f32[16,1,512]{2,1,0:T(1,128)}), f32[16,1,512]{2,1,0:T(1,128)S(1)}, u32[]{:S(2)}, u32[]{:S(2)}) async-start(f32[16,1,512]{2,1,0:T(1,128)} %broadcast_in_dim.17), calls=%async_computation.3 | async-start | bytes 65536 | tf_op jit(solution)/shard_map/all_to_all | solution.py:16
  211.0 21.3 %all-to-all-start.4 = ((bf16[16,128,256]{2,1,0:T(8,128)(2,1)}), bf16[16,128,256]{2,1,0:T(8,128)(2,1)}, u32[]{:S(2)}, u32[]{:S(2)}) async-start(bf16[16,128,256]{2,1,0:T(8,128)(2,1)} %outer.1), calls=%async_computation.4 | async-start | bytes 2097152 | tf_op jit(solution)/shard_map/all_to_all | solution.py:765
  216.2 13.1 %collective-permute-start.33 = (f32[32,128]{1,0:T(8,128)S(1)}, f32[32,128]{1,0:T(8,128)S(1)}, u32[]{:S(2)}, u32[]{:S(2)}) collective-permute-start(f32[32,128]{1,0:T(8,128)S(1)} %slice.46), channel_id=1, source_target_pairs={{16,0},{32,16},{48,32},{64,48},{80,64},{96,80},{112,96},{128,112},... | collective-permute-start | bytes 49160 | tf_op jit(solution)/shard_map/ppermute | solution.py:764
  (35 other events, 530.2 us)
